TPU v7x, 256 devices: a whole 4x4x8 slice. The times are simulated.
256 devices in a mesh: kv: 32 (over z, y), tp: 8 (over x, core).
Axes of the slice: x: 4, y: 4, z: 8, core: 2. Of those that a mesh axis runs over, the one named last changes fastest.
Arguments:
- tokens: bfloat16 [32768, 1024], P('kv', 'tp'), may hold values from -6 to 6
- query_weight: bfloat16 [1024, 2048], P(None, 'tp'), may hold values from -0.1875 to 0.1875
- latent_weight: bfloat16 [1024, 128], replicated, may hold values from -0.1875 to 0.1875
- query_gain: float32 [128], replicated, may hold values from 0.5 to 1.5
- key_gain: float32 [128], replicated, may hold values from 0.5 to 1.5
- value_up: bfloat16 [16, 128, 64], P('tp'), may hold values from -0.5 to 0.5
- out_weight: bfloat16 [1024, 1024], P('tp'), may hold values from -0.25 to 0.25
- out_gain: float32 [1024], replicated, may hold values from 0.5 to 1.5
- chosen: int32 [256, 32], P('kv'), may hold values from -1 to 255, as said below
Outputs:
- mixed_out: bfloat16 [32768, 1024], P('kv', 'tp')
Inputs may be any that keep to these rules, and one draw needn't show every extreme that they name: Row b lists the key blocks chosen for query block b: entry 0 is b itself, then distinct blocks before b, then -1 in every unused place. Block j is held by index j // 8 of kv. All query blocks of one index of kv together choose at most 2 distinct blocks held by any one other index, and some pair of indices reaches that bound; blocks held by the same index are chosen freely.
All inputs are finite; a program needn't handle non-finite values.
Results may differ from a plain program's by a relative error of at most 0.02.
Values may be sent and summed in bfloat16 or wider, within the bound.
A program may use at most 64 MiB of HBM per device.

v0:
```python
import jax
import jax.numpy as jnp
from jax import lax
from jax.sharding import Mesh
from jax.sharding import PartitionSpec as P

BLOCK = 128
PER_OWNER = 2
KV = ("kv_0", "kv_1")


epsilon = 1e-06
masked_score = -1e30


def taken_in(shard, axis, dim, absorb, carry):
    whole = jax.tree.map(lambda part: lax.all_gather(part, axis, axis=dim, tiled=True), shard)
    return absorb(carry, whole, jnp.int32(0))


def split_up(shard, dim, length):
    return jnp.stack(jnp.split(shard, length, axis=dim))


def laid_out(parts, dim):
    lengths = list(parts.shape[1:])
    lengths[dim] *= parts.shape[0]
    return jnp.moveaxis(parts, 0, dim).reshape(lengths)


def exchange_in_order(parts, axes, turns):
    inside = parts.shape[1:]
    result = parts.reshape(*(lax.axis_size(a) for a in axes), *inside)
    for k in turns:
        result = lax.all_to_all(result, axes[k], k, k, tiled=True)
    return result.reshape(-1, *inside)


def one_axis_at_a_time(shard, axes, turns, split_dim, concat_dim):
    parts = split_up(shard, split_dim, lax.axis_size(axes))
    return laid_out(exchange_in_order(parts, axes, turns), concat_dim)


def rms_scale(values, gain_row):
    widened = values.astype(jnp.float32)
    mean_sq = jnp.mean(widened * widened, axis=-1, keepdims=True)
    return (widened * lax.rsqrt(mean_sq + epsilon) * gain_row).astype(jnp.bfloat16)


def shards(
    tokens,
    query_weight,
    latent_weight,
    query_gain,
    key_gain,
    value_up,
    out_weight,
    out_gain,
    chosen,
):
    tok_rows = tokens.shape[0]
    head_cols = query_weight.shape[1]
    lat_width = latent_weight.shape[1]
    local_heads = head_cols // lat_width
    block_size = BLOCK
    blocks_dev = tok_rows // block_size
    owners = lax.axis_size(KV)
    my_owner = lax.axis_index(KV)

    def project(totals, shard_piece, offset):
        query_rows = lax.dynamic_slice_in_dim(query_weight, offset, shard_piece.shape[1], 0)
        latent_rows = lax.dynamic_slice_in_dim(latent_weight, offset, shard_piece.shape[1], 0)
        return (
            totals[0] + jnp.dot(shard_piece, query_rows, preferred_element_type=jnp.float32),
            totals[1] + jnp.dot(shard_piece, latent_rows, preferred_element_type=jnp.float32),
        )

    query_zero = jnp.zeros((tok_rows, head_cols), jnp.float32)
    latent_zero = jnp.zeros((tok_rows, lat_width), jnp.float32)
    query_acc, latent_acc = taken_in(tokens, "tp", 1, project, (query_zero, latent_zero))
    queries = rms_scale(
        query_acc.astype(jnp.bfloat16).reshape(tok_rows, local_heads, lat_width), query_gain
    )
    latent = latent_acc.astype(jnp.bfloat16)
    latent_blocks = latent.reshape(blocks_dev, block_size, lat_width)
    clamped = jnp.maximum(chosen, 0)
    owner_of = clamped // blocks_dev
    index_in = clamped % blocks_dev
    flat_owner = owner_of.reshape(-1)
    flat_index = index_in.reshape(-1)
    remote = (chosen.reshape(-1) >= 0) & (flat_owner != my_owner)
    owner_ids = jnp.arange(owners, dtype=jnp.int32)
    local_ids = jnp.arange(blocks_dev, dtype=jnp.int32)
    matches = (
        remote[:, None, None]
        & (flat_owner[:, None, None] == owner_ids[None, :, None])
        & (flat_index[:, None, None] == local_ids[None, None, :])
    )
    needed = jnp.any(matches, axis=0)
    ranking = jnp.cumsum(needed.astype(jnp.int32), axis=1) - 1
    slot_ids = jnp.arange(PER_OWNER, dtype=jnp.int32)
    placed = needed[:, None, :] & (ranking[:, None, :] == slot_ids[None, :, None])
    wanted = jnp.where(
        jnp.any(placed, axis=2), jnp.sum(jnp.where(placed, local_ids[None, None, :], 0), axis=2), -1
    )
    requested = one_axis_at_a_time(wanted, KV, (0, 1), 0, 0)
    served = latent_blocks[jnp.maximum(requested, 0)]
    served = jnp.where((requested >= 0)[:, :, None, None], served, jnp.zeros_like(served))
    arrived = lax.all_to_all(served, KV, split_axis=0, concat_axis=0, tiled=True)
    block_pool = jnp.concatenate(
        [latent_blocks, arrived.reshape(owners * PER_OWNER, block_size, lat_width)], axis=0
    )
    slot_of = jnp.sum(jnp.where(wanted[owner_of] == index_in[:, :, None], slot_ids, 0), axis=2)
    where_from = jnp.where(
        owner_of == my_owner, index_in, blocks_dev + owner_of * PER_OWNER + slot_of
    )
    selected = block_pool[where_from]
    score_scale = lat_width ** (-0.5)
    offsets = jnp.arange(block_size, dtype=jnp.int32)
    query_blocks = queries.reshape(blocks_dev, block_size, local_heads, lat_width)
    block_starts = my_owner * tok_rows + jnp.arange(blocks_dev, dtype=jnp.int32) * block_size

    def attend(packed):
        query_block, picked_values, chosen_row, start_pos = packed
        picked_keys = rms_scale(picked_values, key_gain)
        scores = (
            jnp.einsum(
                "qhl,ckl->qhck", query_block, picked_keys, preferred_element_type=jnp.float32
            )
            * score_scale
        )
        key_pos = jnp.maximum(chosen_row, 0)[:, None] * block_size + offsets[None, :]
        query_pos = start_pos + offsets
        allowed = (chosen_row[:, None] >= 0)[None] & (key_pos[None] <= query_pos[:, None, None])
        allowed = allowed[:, None]
        scores = jnp.where(allowed, scores, masked_score)
        row_max = jnp.max(scores, axis=(2, 3), keepdims=True)
        exp_scores = jnp.where(allowed, jnp.exp(scores - row_max), 0.0)
        weights = (exp_scores / jnp.sum(exp_scores, axis=(2, 3), keepdims=True)).astype(
            jnp.bfloat16
        )
        attended = jnp.einsum(
            "qhck,ckl->qhl", weights, picked_values, preferred_element_type=jnp.float32
        )
        return attended.astype(jnp.bfloat16)

    attended = lax.map(attend, (query_blocks, selected, chosen, block_starts))
    attended = attended.reshape(tok_rows, local_heads, lat_width)
    heads_out = jnp.einsum("thl,hlv->thv", attended, value_up, preferred_element_type=jnp.float32)
    heads_out = heads_out.astype(jnp.bfloat16).reshape(tok_rows, local_heads * value_up.shape[2])
    model_width = out_weight.shape[1]
    tp_count = lax.axis_size("tp")
    feature_rows = model_width // tp_count
    gain_part = lax.dynamic_slice_in_dim(
        out_gain, lax.axis_index("tp") * feature_rows, feature_rows, 0
    )
    column_block = lax.all_to_all(out_weight, "tp", split_axis=1, concat_axis=0, tiled=True)

    def contract(total, head_piece, offset):
        weight_rows = lax.dynamic_slice_in_dim(column_block, offset, head_piece.shape[1], 0)
        return total + jnp.dot(head_piece, weight_rows, preferred_element_type=jnp.float32)

    empty_cols = jnp.zeros((tok_rows, feature_rows), jnp.float32)
    summed = taken_in(heads_out, "tp", 1, contract, empty_cols)
    squares = lax.psum(jnp.sum(summed * summed, axis=1), "tp")
    mixed_out = (summed * lax.rsqrt(squares / model_width + epsilon)[:, None] * gain_part).astype(
        jnp.bfloat16
    )
    return mixed_out


def solution(mesh):
    torus = Mesh(mesh.devices.reshape(8, 4, mesh.shape["tp"]), ("kv_0", "kv_1", "tp"))
    in_specs = (
        P(KV, "tp"),
        P(None, "tp"),
        P(),
        P(),
        P(),
        P("tp", None, None),
        P("tp", None),
        P(),
        P(KV, None),
    )
    out_specs = P(KV, "tp")
    return jax.shard_map(
        shards, mesh=torus, in_specs=in_specs, out_specs=out_specs, check_vma=False
    )
```

profile of v0, /device:TPU:1, one launch (start us, length us, event | category | flops | bytes accessed | tf_op | source)
XLA Modules:
  0.0 257.7 jit_solution(599422466508206206)
XLA Ops:
  13.4 15.4 %all_to_all.34 = s32[8,4,1,2]{1,3,2,0:T(2,128)S(1)} all-to-all(s32[8,4,1,2]{1,3,2,0:T(2,128)S(1)} %copy.165), channel_id=1, replica_groups=mesh['kv_0'=8,'kv_1'=4,'tp'=8] {'kv_0'}, dimensions={0} | all-to-all | bytes 512 | tf_op jit(solution)/shard_map/all_to_all | solution.py:35
  28.8 8.1 %all_to_all.35 = s32[8,4,1,2]{0,3,2,1:T(2,128)S(1)} all-to-all(s32[8,4,1,2]{0,3,2,1:T(2,128)S(1)} %copy.166), channel_id=1, replica_groups=mesh['kv_0'=8,'kv_1'=4,'tp'=8] {'kv_1'}, dimensions={1} | all-to-all | bytes 512 | tf_op jit(solution)/shard_map/all_to_all | solution.py:35
  37.3 5.2 %all-gather.3.cloned.1.call-done = bf16[1024,1024]{1,0:T(8,128)(2,1)} async-done(((bf16[1024,128]{1,0:T(8,128)(2,1)}), bf16[1024,1024]{1,0:T(8,128)(2,1)}) %all-gather.3.cloned.1.call-update) | async-done | bytes 2097168 | tf_op jit(solution)/shard_map/all_gather | solution.py:17
  42.5 2.3 convolution_convert_fusion.2
  47.4 9.4 %all-to-all-start.2 = ((bf16[32,2,128,128]{3,2,1,0:T(8,128)(2,1)}), bf16[32,2,128,128]{3,2,1,0:T(8,128)(2,1)S(1)}, u32[]{:S(2)}, u32[]{:S(2)}) async-start(bf16[32,2,128,128]{3,2,1,0:T(8,128)(2,1)} %broadcast_select_fusion), calls=%async_computation.2 | async-start | bytes 4194304 | tf_op jit(solution)/shard_map/all_to_all | solution.py:109
  58.3 2.4 bitcast_reduce_fusion
  62.0 2.5 copy.128
  64.6 2.4 multiply_convert_fusion.1
  67.0 38.7 %all-to-all-done.2 = bf16[32,2,128,128]{3,2,1,0:T(8,128)(2,1)S(1)} async-done(((bf16[32,2,128,128]{3,2,1,0:T(8,128)(2,1)}), bf16[32,2,128,128]{3,2,1,0:T(8,128)(2,1)S(1)}, u32[]{:S(2)}, u32[]{:S(2)}) %all-to-all-start.2) | async-done | bytes 2097184 | tf_op jit(solution)/shard_map/all_to_all | solution.py:109
  108.8 8.3 %gather_fusion.2 = bf16[256,128,128]{2,1,0:T(8,128)(2,1)} fusion(bf16[72,128,128]{2,1,0:T(8,128)(2,1)S(1)} %pad_maximum_fusion, s32[1024]{0:T(1024)S(1)} %pad_clamp_fusion), kind=kCustom, calls=%fused_computation.2 | custom fusion | bytes 16778240 | tf_op jit(solution)/shard_map/gather | solution.py:117
  117.1 88.6 %while.12 = (s32[]{:T(128)}, bf16[8,128,2,128]{3,1,0,2:T(8,128)(2,1)}, s32[8,32]{1,0:T(8,128)S(1)}, s32[8]{0:T(128)S(1)}, bf16[8,128,2,128]{3,1,2,0:T(8,128)(2,1...) while((s32[]{:T(128)}, ...), condition=%wide.region_10.11_spmd.clone.clone, body=%wide.region_6.10_spmd.clone.clone.sunk | while | flops 556310272 | bytes 18064560 | solution.py:147
  121.2 2.4 fusion.41
  124.6 3.6 %fusion.43 = bf16[8,128,2,128]{3,1,0,2:T(8,128)(2,1)} fusion(bf16[8,128,2,128]{3,1,0,2:T(8,128)(2,1)} %get-tuple-element.198, s32[]{:T(128)} %get-tuple-element.197, f32[128,2,32,128]{0,3,2,1:T(8,128)S(1)} %get-tuple-element.187, f32[128,2]{0,1:T(2,128)S(1)} %fusion.42, f32[128,2]{0,1:T(2,128)S(1)} %get-tuple-element.188, ...), kind=kOutput, calls=%fused_computation.16.clone.1 | convolution fusion | flops 274759680 | bytes 5835776 | tf_op jit(solution)/shard_map/while/body/eval_jaxpr/qhck,ckl->qhl/dot_general | solution.py:142
  132.2 2.4 fusion.41
  135.7 3.6 %fusion.43 = bf16[8,128,2,128]{3,1,0,2:T(8,128)(2,1)} fusion(bf16[8,128,2,128]{3,1,0,2:T(8,128)(2,1)} %get-tuple-element.198, s32[]{:T(128)} %get-tuple-element.197, f32[128,2,32,128]{0,3,2,1:T(8,128)S(1)} %get-tuple-element.187, f32[128,2]{0,1:T(2,128)S(1)} %fusion.42, f32[128,2]{0,1:T(2,128)S(1)} %get-tuple-element.188, ...), kind=kOutput, calls=%fused_computation.16.clone.1 | convolution fusion | flops 274759680 | bytes 5835776 | tf_op jit(solution)/shard_map/while/body/eval_jaxpr/qhck,ckl->qhl/dot_general | solution.py:142
  143.3 2.4 fusion.41
  146.8 3.6 %fusion.43 = bf16[8,128,2,128]{3,1,0,2:T(8,128)(2,1)} fusion(bf16[8,128,2,128]{3,1,0,2:T(8,128)(2,1)} %get-tuple-element.198, s32[]{:T(128)} %get-tuple-element.197, f32[128,2,32,128]{0,3,2,1:T(8,128)S(1)} %get-tuple-element.187, f32[128,2]{0,1:T(2,128)S(1)} %fusion.42, f32[128,2]{0,1:T(2,128)S(1)} %get-tuple-element.188, ...), kind=kOutput, calls=%fused_computation.16.clone.1 | convolution fusion | flops 274759680 | bytes 5835776 | tf_op jit(solution)/shard_map/while/body/eval_jaxpr/qhck,ckl->qhl/dot_general | solution.py:142
  154.4 2.4 fusion.41
  157.9 3.6 %fusion.43 = bf16[8,128,2,128]{3,1,0,2:T(8,128)(2,1)} fusion(bf16[8,128,2,128]{3,1,0,2:T(8,128)(2,1)} %get-tuple-element.198, s32[]{:T(128)} %get-tuple-element.197, f32[128,2,32,128]{0,3,2,1:T(8,128)S(1)} %get-tuple-element.187, f32[128,2]{0,1:T(2,128)S(1)} %fusion.42, f32[128,2]{0,1:T(2,128)S(1)} %get-tuple-element.188, ...), kind=kOutput, calls=%fused_computation.16.clone.1 | convolution fusion | flops 274759680 | bytes 5835776 | tf_op jit(solution)/shard_map/while/body/eval_jaxpr/qhck,ckl->qhl/dot_general | solution.py:142
  165.5 2.4 fusion.41
  168.9 3.6 %fusion.43 = bf16[8,128,2,128]{3,1,0,2:T(8,128)(2,1)} fusion(bf16[8,128,2,128]{3,1,0,2:T(8,128)(2,1)} %get-tuple-element.198, s32[]{:T(128)} %get-tuple-element.197, f32[128,2,32,128]{0,3,2,1:T(8,128)S(1)} %get-tuple-element.187, f32[128,2]{0,1:T(2,128)S(1)} %fusion.42, f32[128,2]{0,1:T(2,128)S(1)} %get-tuple-element.188, ...), kind=kOutput, calls=%fused_computation.16.clone.1 | convolution fusion | flops 274759680 | bytes 5835776 | tf_op jit(solution)/shard_map/while/body/eval_jaxpr/qhck,ckl->qhl/dot_general | solution.py:142
  176.5 2.4 fusion.41
  180.0 3.6 %fusion.43 = bf16[8,128,2,128]{3,1,0,2:T(8,128)(2,1)} fusion(bf16[8,128,2,128]{3,1,0,2:T(8,128)(2,1)} %get-tuple-element.198, s32[]{:T(128)} %get-tuple-element.197, f32[128,2,32,128]{0,3,2,1:T(8,128)S(1)} %get-tuple-element.187, f32[128,2]{0,1:T(2,128)S(1)} %fusion.42, f32[128,2]{0,1:T(2,128)S(1)} %get-tuple-element.188, ...), kind=kOutput, calls=%fused_computation.16.clone.1 | convolution fusion | flops 274759680 | bytes 5835776 | tf_op jit(solution)/shard_map/while/body/eval_jaxpr/qhck,ckl->qhl/dot_general | solution.py:142
  187.6 2.4 fusion.41
  191.1 3.6 %fusion.43 = bf16[8,128,2,128]{3,1,0,2:T(8,128)(2,1)} fusion(bf16[8,128,2,128]{3,1,0,2:T(8,128)(2,1)} %get-tuple-element.198, s32[]{:T(128)} %get-tuple-element.197, f32[128,2,32,128]{0,3,2,1:T(8,128)S(1)} %get-tuple-element.187, f32[128,2]{0,1:T(2,128)S(1)} %fusion.42, f32[128,2]{0,1:T(2,128)S(1)} %get-tuple-element.188, ...), kind=kOutput, calls=%fused_computation.16.clone.1 | convolution fusion | flops 274759680 | bytes 5835776 | tf_op jit(solution)/shard_map/while/body/eval_jaxpr/qhck,ckl->qhl/dot_general | solution.py:142
  198.7 2.4 fusion.41
  202.2 3.6 %fusion.43 = bf16[8,128,2,128]{3,1,0,2:T(8,128)(2,1)} fusion(bf16[8,128,2,128]{3,1,0,2:T(8,128)(2,1)} %get-tuple-element.198, s32[]{:T(128)} %get-tuple-element.197, f32[128,2,32,128]{0,3,2,1:T(8,128)S(1)} %get-tuple-element.187, f32[128,2]{0,1:T(2,128)S(1)} %fusion.42, f32[128,2]{0,1:T(2,128)S(1)} %get-tuple-element.188, ...), kind=kOutput, calls=%fused_computation.16.clone.1 | convolution fusion | flops 274759680 | bytes 5835776 | tf_op jit(solution)/shard_map/while/body/eval_jaxpr/qhck,ckl->qhl/dot_general | solution.py:142
  208.7 6.6 %all-to-all-start.3 = ((bf16[128,8,128]{0,2,1:T(8,128)(2,1)}), bf16[128,8,128]{0,2,1:T(8,128)(2,1)S(1)}, u32[]{:S(2)}, u32[]{:S(2)}) async-start(bf16[128,8,128]{0,2,1:T(8,128)(2,1)} %bitcast.43), calls=%async_computation.3 | async-start | bytes 524288 | tf_op jit(solution)/shard_map/all_to_all | solution.py:157
  216.0 5.7 %all-to-all-done.3 = bf16[128,8,128]{0,2,1:T(8,128)(2,1)S(1)} async-done(((bf16[128,8,128]{0,2,1:T(8,128)(2,1)}), bf16[128,8,128]{0,2,1:T(8,128)(2,1)S(1)}, u32[]{:S(2)}, u32[]{:S(2)}) %all-to-all-start.3) | async-done | bytes 262176 | tf_op jit(solution)/shard_map/all_to_all | solution.py:157
  221.9 13.8 %all-gather.5.cloned.1.call-done = bf16[1024,1024]{0,1:T(8,128)(2,1)} async-done(((bf16[1024,128]{0,1:T(8,128)(2,1)}), bf16[1024,1024]{0,1:T(8,128)(2,1)}) %all-gather.5.cloned.1.call-update) | async-done | bytes 2097168 | tf_op jit(solution)/shard_map/all_gather | solution.py:17
  235.8 2.1 multiply_reduce_fusion.1
  237.9 12.1 %psum.7 = f32[1024]{0:T(1024)S(1)} all-reduce(f32[1024]{0:T(1024)S(1)} %get-tuple-element.140), channel_id=1, replica_groups=mesh['kv_0'=8,'kv_1'=4,'tp'=8] {'tp'}, use_global_device_ids=true, to_apply=%region_12.13 | all-reduce | flops 1024 | bytes 8192 | tf_op jit(solution)/shard_map/psum | solution.py:165
  (175 shorter events, 61.2 us)
Async XLA Ops:
  6.5 51.8 %copy-start = (bf16[1024,256]{1,0:T(8,128)(2,1)S(1)}, bf16[1024,256]{1,0:T(8,128)(2,1)}, u32[]{:S(2)}) copy-start(bf16[1024,256]{1,0:T(8,128)(2,1)} %param.12) | copy-start | bytes 1572868
  6.5 36.0 %all-gather.3.cloned.1.call-start = ((), (), s32[]{:S(2)}) async-start(), calls=%async_computation.4 | async-start | bytes 2359296 | tf_op jit(solution)/shard_map/all_gather | solution.py:17
  45.8 12.4 %copy-start.3 = (s32[8,32]{1,0:T(8,128)S(1)}, s32[8,32]{1,0:T(8,128)}, u32[]{:S(2)}) copy-start(s32[8,32]{1,0:T(8,128)} %param.19) | copy-start | bytes 3076
  47.4 58.3 %all-to-all-start.2 = ((bf16[32,2,128,128]{3,2,1,0:T(8,128)(2,1)}), bf16[32,2,128,128]{3,2,1,0:T(8,128)(2,1)S(1)}, u32[]{:S(2)}, u32[]{:S(2)}) async-start(bf16[32,2,128,128]{3,2,1,0:T(8,128)(2,1)} %broadcast_select_fusion), calls=%async_computation.2 | async-start | bytes 4194304 | tf_op jit(solution)/shard_map/all_to_all | solution.py:109
  56.8 178.9 %all-gather.5.cloned.1.call-start = ((), (), s32[]{:S(2)}) async-start(), calls=%async_computation.5 | async-start | bytes 2359296 | tf_op jit(solution)/shard_map/all_gather | solution.py:17
  58.3 6.2 %copy-start.5 = (f32[128]{0:T(128)S(1)}, f32[128]{0:T(128)}, u32[]{:S(2)}) copy-start(f32[128]{0:T(128)} %param.14) | copy-start | bytes 1540
  105.7 1.4 copy-start.1
  108.8 8.3 %copy-start.6 = (f32[128]{0:T(128)S(1)}, f32[128]{0:T(128)}, u32[]{:S(2)}) copy-start(f32[128]{0:T(128)} %param.15) | copy-start | bytes 1540
  117.1 88.6 %copy-start.4 = (bf16[2,128,64]{1,2,0:T(8,128)(2,1)S(1)}, bf16[2,128,64]{1,2,0:T(8,128)(2,1)}, u32[]{:S(2)}) copy-start(bf16[2,128,64]{1,2,0:T(8,128)(2,1)} %param.16) | copy-start | bytes 98308
  117.1 90.7 %copy-start.2 = (bf16[128,1024]{1,0:T(8,128)(2,1)S(1)}, bf16[128,1024]{1,0:T(8,128)(2,1)}, u32[]{:S(2)}) copy-start(bf16[128,1024]{1,0:T(8,128)(2,1)} %param.17) | copy-start | bytes 786436
  208.7 13.1 %all-to-all-start.3 = ((bf16[128,8,128]{0,2,1:T(8,128)(2,1)}), bf16[128,8,128]{0,2,1:T(8,128)(2,1)S(1)}, u32[]{:S(2)}, u32[]{:S(2)}) async-start(bf16[128,8,128]{0,2,1:T(8,128)(2,1)} %bitcast.43), calls=%async_computation.3 | async-start | bytes 524288 | tf_op jit(solution)/shard_map/all_to_all | solution.py:157
Sparse Core Ops, SparseCore 0:
  9.2 33.3 all-gather.2
  207.9 27.7 all-gather.4
where the time goes:
time: 259 us; the launch traced here: 258 us
  waiting for transfers between devices  64.2 us (25%)
  matrix products  56.2 us (22%)
  other arithmetic  44.3 us (17%)
  blocking collectives  35.6 us (14%)
  local copies, waits for them, and re-layouts  27.2 us (11%)
  starting transfers between devices  16.2 us (6%)
  between operations  13.6 us (5%)
    all_to_all x1, waiting for transfers between devices, shards(): lax.all_to_all(served, KV, split_axis=0, concat_axis=0, tiled=True)  38.7 us
    dot_general x8, matrix products, attend(): jnp.einsum('qhck,ckl->qhl', weights, picked_values, preferred_element_typ...  28.6 us
    all_to_all x2, blocking collectives, exchange_in_order(): result = lax.all_to_all(result, axes[k], k, k, tiled=True)  23.5 us
    all_gather x2, waiting for transfers between devices, taken_in(): lax.all_gather(part, axis, axis=dim, tiled=True)  19.1 us
    dot_general x8, matrix products, attend(): jnp.einsum('qhl,ckl->qhck', query_block, picked_keys, preferred_element_t...  18.9 us
    reduce_sum x8, other arithmetic, rms_scale(): mean_sq = jnp.mean(widened * widened, axis=-1, keepdims=True)  14.7 us
    psum x1, blocking collectives, shards(): squares = lax.psum(jnp.sum(summed * summed, axis=1), 'tp')  12.1 us
    all_to_all x1, starting transfers between devices, shards(): lax.all_to_all(served, KV, split_axis=0, concat_axis=0, tiled=True)  9.45 us
  transfers between devices with their start and end apart: 4, of which 4 were waited for; matrix products, arithmetic and copies ran while one was open for 7% of the time, Pallas kernels for 0%

commit v1 on v0

--- a/solution.py
+++ b/solution.py
@@ -1,12 +1,16 @@
 import jax
 import jax.numpy as jnp
 from jax import lax
+from jax.experimental import pallas as pl
+from jax.experimental.pallas import tpu as pltpu
 from jax.sharding import Mesh
 from jax.sharding import PartitionSpec as P
 
 BLOCK = 128
 PER_OWNER = 2
 KV = ("kv_0", "kv_1")
+GROUP = 8
+LOG2E = 1.4426950408889634
 
 
 epsilon = 1e-06
@@ -41,10 +45,87 @@
     return laid_out(exchange_in_order(parts, axes, turns), concat_dim)
 
 
-def rms_scale(values, gain_row):
-    widened = values.astype(jnp.float32)
-    mean_sq = jnp.mean(widened * widened, axis=-1, keepdims=True)
-    return (widened * lax.rsqrt(mean_sq + epsilon) * gain_row).astype(jnp.bfloat16)
+def attend_block(slots_ref, query_ref, pool_ref, query_gain_ref, key_gain_ref, up_ref, out_ref, keys, values):
+    step = pl.program_id(0)
+    width = pool_ref.shape[1]
+    heads = up_ref.shape[0]
+    picks = slots_ref.shape[1]
+    pool_rows = pool_ref.shape[0]
+
+    @pl.when(step == 0)
+    def _():
+        def prepare(j, carry):
+            rows = pl.ds(pl.multiple_of(j * 2 * BLOCK, 2 * BLOCK), 2 * BLOCK)
+            latent = pool_ref[rows, :]
+            wide = latent.astype(jnp.float32)
+            mean_sq = jnp.mean(wide * wide, axis=-1, keepdims=True)
+            keys[rows, :] = (wide * lax.rsqrt(mean_sq + epsilon) * key_gain_ref[...]).astype(jnp.bfloat16)
+            values[rows, :width] = latent
+            values[rows, width:] = jnp.ones((2 * BLOCK, width), jnp.bfloat16)
+            return carry
+
+        lax.fori_loop(0, pool_rows // (2 * BLOCK), prepare, 0)
+        keys[pool_rows:, :] = jnp.zeros((BLOCK, width), jnp.bfloat16)
+        values[pool_rows:, :] = jnp.zeros((BLOCK, 2 * width), jnp.bfloat16)
+
+    scale = width ** (-0.5) * LOG2E
+    parts = []
+    for h in range(heads):
+        wide = query_ref[:, h * width : (h + 1) * width].astype(jnp.float32)
+        mean_sq = jnp.mean(wide * wide, axis=-1, keepdims=True)
+        parts.append((wide * lax.rsqrt(mean_sq + epsilon) * (query_gain_ref[...] * scale)).astype(jnp.bfloat16))
+    queries = jnp.concatenate(parts, axis=0)
+
+    def rows_of(c):
+        return pl.ds(pl.multiple_of(slots_ref[step, c] * BLOCK, BLOCK), BLOCK)
+
+    def group(first, masked):
+        places = [rows_of(first + i) for i in range(GROUP)]
+        picked = jnp.concatenate([keys[r, :] for r in places], axis=0)
+        scores = lax.dot_general(
+            queries, picked, (((1,), (1,)), ((), ())), preferred_element_type=jnp.float32
+        )
+        if masked:
+            row = lax.broadcasted_iota(jnp.int32, scores.shape, 0) % BLOCK
+            col = lax.broadcasted_iota(jnp.int32, scores.shape, 1)
+            scores = jnp.where((col <= row) | (col >= BLOCK), scores, masked_score)
+        weights = jnp.exp2(scores).astype(jnp.bfloat16)
+        held = jnp.concatenate([values[r, :] for r in places], axis=0)
+        return jnp.dot(weights, held, preferred_element_type=jnp.float32)
+
+    total = group(0, True)
+    total = lax.fori_loop(1, picks // GROUP, lambda g, t: t + group(g * GROUP, False), total)
+    attended = (total[:, :width] / total[:, width:]).astype(jnp.bfloat16)
+    outs = [
+        jnp.dot(attended[h * BLOCK : (h + 1) * BLOCK], up_ref[h], preferred_element_type=jnp.float32)
+        for h in range(heads)
+    ]
+    out_ref[...] = jnp.concatenate(outs, axis=1).astype(jnp.bfloat16)
+
+
+def attention(slots, queries, pool, query_gain, key_gain, value_up):
+    rows, cols = queries.shape
+    pool_rows, width = pool.shape
+    heads, _, vdim = value_up.shape
+    whole = pl.BlockSpec(memory_space=pltpu.VMEM)
+    return pl.pallas_call(
+        attend_block,
+        grid=(rows // BLOCK,),
+        out_shape=jax.ShapeDtypeStruct((rows, heads * vdim), jnp.bfloat16),
+        in_specs=[
+            pl.BlockSpec(memory_space=pltpu.SMEM),
+            pl.BlockSpec((BLOCK, cols), lambda b: (b, 0)),
+            whole,
+            whole,
+            whole,
+            whole,
+        ],
+        out_specs=pl.BlockSpec((BLOCK, heads * vdim), lambda b: (b, 0)),
+        scratch_shapes=[
+            pltpu.VMEM((pool_rows + BLOCK, width), jnp.bfloat16),
+            pltpu.VMEM((pool_rows + BLOCK, 2 * width), jnp.bfloat16),
+        ],
+    )(slots, queries, pool, query_gain, key_gain, value_up)
 
 
 def shards(
@@ -78,9 +159,6 @@
     query_zero = jnp.zeros((tok_rows, head_cols), jnp.float32)
     latent_zero = jnp.zeros((tok_rows, lat_width), jnp.float32)
     query_acc, latent_acc = taken_in(tokens, "tp", 1, project, (query_zero, latent_zero))
-    queries = rms_scale(
-        query_acc.astype(jnp.bfloat16).reshape(tok_rows, local_heads, lat_width), query_gain
-    )
     latent = latent_acc.astype(jnp.bfloat16)
     latent_blocks = latent.reshape(blocks_dev, block_size, lat_width)
     clamped = jnp.maximum(chosen, 0)
@@ -114,40 +192,16 @@
     where_from = jnp.where(
         owner_of == my_owner, index_in, blocks_dev + owner_of * PER_OWNER + slot_of
     )
-    selected = block_pool[where_from]
-    score_scale = lat_width ** (-0.5)
-    offsets = jnp.arange(block_size, dtype=jnp.int32)
-    query_blocks = queries.reshape(blocks_dev, block_size, local_heads, lat_width)
-    block_starts = my_owner * tok_rows + jnp.arange(blocks_dev, dtype=jnp.int32) * block_size
-
-    def attend(packed):
-        query_block, picked_values, chosen_row, start_pos = packed
-        picked_keys = rms_scale(picked_values, key_gain)
-        scores = (
-            jnp.einsum(
-                "qhl,ckl->qhck", query_block, picked_keys, preferred_element_type=jnp.float32
-            )
-            * score_scale
-        )
-        key_pos = jnp.maximum(chosen_row, 0)[:, None] * block_size + offsets[None, :]
-        query_pos = start_pos + offsets
-        allowed = (chosen_row[:, None] >= 0)[None] & (key_pos[None] <= query_pos[:, None, None])
-        allowed = allowed[:, None]
-        scores = jnp.where(allowed, scores, masked_score)
-        row_max = jnp.max(scores, axis=(2, 3), keepdims=True)
-        exp_scores = jnp.where(allowed, jnp.exp(scores - row_max), 0.0)
-        weights = (exp_scores / jnp.sum(exp_scores, axis=(2, 3), keepdims=True)).astype(
-            jnp.bfloat16
-        )
-        attended = jnp.einsum(
-            "qhck,ckl->qhl", weights, picked_values, preferred_element_type=jnp.float32
-        )
-        return attended.astype(jnp.bfloat16)
-
-    attended = lax.map(attend, (query_blocks, selected, chosen, block_starts))
-    attended = attended.reshape(tok_rows, local_heads, lat_width)
-    heads_out = jnp.einsum("thl,hlv->thv", attended, value_up, preferred_element_type=jnp.float32)
-    heads_out = heads_out.astype(jnp.bfloat16).reshape(tok_rows, local_heads * value_up.shape[2])
+    pool_count = block_pool.shape[0]
+    slots = jnp.where(chosen >= 0, where_from, pool_count).astype(jnp.int32)
+    heads_out = attention(
+        slots,
+        query_acc.astype(jnp.bfloat16),
+        block_pool.reshape(pool_count * block_size, lat_width),
+        query_gain.reshape(1, lat_width),
+        key_gain.reshape(1, lat_width),
+        value_up,
+    )
     model_width = out_weight.shape[1]
     tp_count = lax.axis_size("tp")
     feature_rows = model_width // tp_count

time: 259 us -> 187 us (0.72)
  matrix products: 56.2 us -> 7.81 us
  other arithmetic: 44.3 us -> 6.42 us
  Pallas kernels: 0 us -> 27.2 us
  local copies, waits for them, and re-layouts: 27.2 us -> 9.33 us
  waiting for transfers between devices: 64.2 us -> 69.8 us
    dot_general x17 -> x0, matrix products: 49.5 us -> none  [the longest x8 28.6 us: attend(): jnp.einsum('qhck,ckl->qhl', weights, picked_values, preferred_element_typ...]
    pallas_call x0 -> x1, Pallas kernels: none -> 27.2 us  [attention(): pl.pallas_call(attend_block, grid=(rows // BLOCK,), out_shape=jax.ShapeDt...]
    reduce_sum x16 -> x0, other arithmetic: 23.6 us -> none  [the longest x8 14.7 us: rms_scale(): mean_sq = jnp.mean(widened * widened, axis=-1, keepdims=True)]
    gather x1 -> x0, local copies, waits for them, and re-layouts: 8.28 us -> none  [shards(): selected = block_pool[where_from]]
    and x8 -> x0, other arithmetic: 6.28 us -> none  [attend(): (chosen_row[:, None] >= 0)[None]]
    add x17 -> x0, other arithmetic: 5.61 us -> none  [the longest x8 5.02 us: attend(): query_pos = start_pos + offsets]
    dynamic_slice x8 -> x0, local copies, waits for them, and re-layouts: 5.12 us -> none  [shards(): attended = lax.map(attend, (query_blocks, selected, chosen, block_starts))]
    all_to_all x1, waiting for transfers between devices: 38.7 us -> 43.2 us  [shards(): lax.all_to_all(served, KV, split_axis=0, concat_axis=0, tiled=True)]
where the time goes in v1:
time: 187 us; the launch traced here: 186 us
  waiting for transfers between devices  69.8 us (37%)
  blocking collectives  35.6 us (19%)
  Pallas kernels  27.2 us (15%)
  starting transfers between devices  16.2 us (9%)
  between operations  13.6 us (7%)
  local copies, waits for them, and re-layouts  9.33 us (5%)
  matrix products  7.81 us (4%)
  other arithmetic  6.42 us (3%)
    all_to_all x1, waiting for transfers between devices, shards(): lax.all_to_all(served, KV, split_axis=0, concat_axis=0, tiled=True)  43.2 us
    pallas_call x1, Pallas kernels, attention(): pl.pallas_call(attend_block, grid=(rows // BLOCK,), out_shape=jax.ShapeDt...  27.2 us
    all_to_all x2, blocking collectives, exchange_in_order(): result = lax.all_to_all(result, axes[k], k, k, tiled=True)  23.5 us
    all_gather x2, waiting for transfers between devices, taken_in(): lax.all_gather(part, axis, axis=dim, tiled=True)  20 us
    psum x1, blocking collectives, shards(): squares = lax.psum(jnp.sum(summed * summed, axis=1), 'tp')  12 us
    all_to_all x1, starting transfers between devices, shards(): lax.all_to_all(served, KV, split_axis=0, concat_axis=0, tiled=True)  9.58 us
    all_to_all x1, starting transfers between devices, shards(): lax.all_to_all(out_weight, 'tp', split_axis=1, concat_axis=0, tiled=True)  6.55 us
    all_to_all x1, waiting for transfers between devices, shards(): lax.all_to_all(out_weight, 'tp', split_axis=1, concat_axis=0, tiled=True)  5.74 us
  transfers between devices with their start and end apart: 4, of which 4 were waited for; matrix products, arithmetic and copies ran while one was open for 7% of the time, Pallas kernels for 0%

profile of v1, /device:TPU:1, one launch (start us, length us, event | category | flops | bytes accessed | tf_op | source)
XLA Modules:
  0.0 185.8 jit_solution(10175384494903397216)
XLA Ops:
  6.5 0.7 all-gather.3.cloned.1.call-update
  7.3 0.7 compare_select_fusion
  8.1 0.7 broadcast_compare_fusion
  8.9 0.6 and_reduce_fusion
  9.7 0.2 reduce_window_sum.11
  13.1 0.1 stack.131
  13.4 15.4 %all_to_all.34 = s32[8,4,1,2]{1,3,2,0:T(2,128)S(1)} all-to-all(s32[8,4,1,2]{1,3,2,0:T(2,128)S(1)} %copy.149), channel_id=1, replica_groups=mesh['kv_0'=8,'kv_1'=4,'tp'=8] {'kv_0'}, dimensions={0} | all-to-all | bytes 512 | tf_op jit(solution)/shard_map/all_to_all | solution.py:39
  28.8 8.1 %all_to_all.35 = s32[8,4,1,2]{0,3,2,1:T(2,128)S(1)} all-to-all(s32[8,4,1,2]{0,3,2,1:T(2,128)S(1)} %copy.150), channel_id=1, replica_groups=mesh['kv_0'=8,'kv_1'=4,'tp'=8] {'kv_1'}, dimensions={1} | all-to-all | bytes 512 | tf_op jit(solution)/shard_map/all_to_all | solution.py:39
  37.1 0.1 reshape.157
  37.2 0.1 copy.160
  37.3 5.2 %all-gather.3.cloned.1.call-done = bf16[1024,1024]{1,0:T(8,128)(2,1)} async-done(((bf16[1024,128]{1,0:T(8,128)(2,1)}), bf16[1024,1024]{1,0:T(8,128)(2,1)}) %all-gather.3.cloned.1.call-update) | async-done | bytes 2097168 | tf_op jit(solution)/shard_map/all_gather | solution.py:21
  42.5 2.3 %convolution_convert_fusion.1 = bf16[1024,128]{1,0:T(8,128)(2,1)S(1)} fusion(bf16[1024,1024]{1,0:T(8,128)(2,1)} %all-gather.3.cloned.1.call-done, bf16[1024,128]{1,0:T(8,128)(2,1)} %param.11), kind=kOutput, calls=%fused_computation.5 | convolution fusion | flops 268566528 | bytes 2621440 | tf_op jit(solution)/shard_map/dot_general | solution.py:156
  44.8 1.0 gather_fusion.1
  45.8 1.5 broadcast_select_fusion
  47.3 9.6 %all-to-all-start.2 = ((bf16[32,2,128,128]{3,2,1,0:T(8,128)(2,1)}), bf16[32,2,128,128]{3,2,1,0:T(8,128)(2,1)S(1)}, u32[]{:S(2)}, u32[]{:S(2)}) async-start(bf16[32,2,128,128]{3,2,1,0:T(8,128)(2,1)} %broadcast_select_fusion), calls=%async_computation.2 | async-start | bytes 4194304 | tf_op jit(solution)/shard_map/all_to_all | solution.py:187
  57.0 0.7 gather_fusion
  57.8 0.7 copy.156.up_ref
  58.5 0.3 select_reduce_fusion
  58.8 0.6 select_select_fusion.slots_ref
  59.4 3.1 %convolution_convert_fusion.query_ref = bf16[1024,256]{1,0:T(8,128)(2,1)} fusion(bf16[1024,1024]{1,0:T(8,128)(2,1)} %all-gather.3.cloned.1.call-done, bf16[1024,256]{1,0:T(8,128)(2,1)S(1)} %copy-done), kind=kOutput, calls=%fused_computation.4 | convolution fusion | flops 537133056 | bytes 3145728 | tf_op jit(solution)/shard_map/dot_general | solution.py:155
  62.5 43.2 %all-to-all-done.2 = bf16[32,2,128,128]{3,2,1,0:T(8,128)(2,1)S(1)} async-done(((bf16[32,2,128,128]{3,2,1,0:T(8,128)(2,1)}), bf16[32,2,128,128]{3,2,1,0:T(8,128)(2,1)S(1)}, u32[]{:S(2)}, u32[]{:S(2)}) %all-to-all-start.2) | async-done | bytes 2097184 | tf_op jit(solution)/shard_map/all_to_all | solution.py:187
  105.7 1.6 pad_maximum_fusion
  107.4 27.2 %shard_map.91 = bf16[1024,128]{1,0:T(8,128)(2,1)} custom-call(s32[8,32]{1,0:T(8,128)} %select_select_fusion.slots_ref, bf16[1024,256]{1,0:T(8,128)(2,1)} %convolution_convert_fusion.query_ref, bf16[9216,128]{1,0:T(8,128)(2,1)} %bitcast.87, f32[1,128]{1,0:T(1,128)} %bitcast.94, f32[1,128]{1,0:T(1,128)} %bitcast.95, bf16[2,128,64]{2,1,0:T(8,128)(2,1)} %copy.156.up_ref), custom_call_target="tpu_custom_call" | custom-call | tf_op jit(solution)/shard_map/pallas_call | solution.py:111
  134.6 0.9 copy.157
  135.4 6.5 %all-to-all-start.3 = ((bf16[128,8,128]{0,2,1:T(8,128)(2,1)}), bf16[128,8,128]{0,2,1:T(8,128)(2,1)S(1)}, u32[]{:S(2)}, u32[]{:S(2)}) async-start(bf16[128,8,128]{0,2,1:T(8,128)(2,1)} %bitcast.40), calls=%async_computation.3 | async-start | bytes 524288 | tf_op jit(solution)/shard_map/all_to_all | solution.py:211
  142.0 0.8 dynamic_slice.3
  142.7 5.7 %all-to-all-done.3 = bf16[128,8,128]{0,2,1:T(8,128)(2,1)S(1)} async-done(((bf16[128,8,128]{0,2,1:T(8,128)(2,1)}), bf16[128,8,128]{0,2,1:T(8,128)(2,1)S(1)}, u32[]{:S(2)}, u32[]{:S(2)}) %all-to-all-start.3) | async-done | bytes 262176 | tf_op jit(solution)/shard_map/all_to_all | solution.py:211
  148.5 0.2 copy.158
  148.7 14.8 %all-gather.5.cloned.1.call-done = bf16[1024,1024]{1,0:T(8,128)(2,1)} async-done(((bf16[1024,128]{1,0:T(8,128)(2,1)}), bf16[1024,1024]{1,0:T(8,128)(2,1)}) %all-gather.5.cloned.1.call-update) | async-done | bytes 2097168 | tf_op jit(solution)/shard_map/all_gather | solution.py:21
  163.5 2.4 %multiply_reduce_fusion = (f32[1024]{0:T(1024)S(1)}, f32[1024,128]{0,1:T(8,128)S(1)}) fusion(bf16[1024,1024]{1,0:T(8,128)(2,1)} %all-gather.5.cloned.1.call-done, bf16[1024,128]{1,0:T(8,128)(2,1)S(1)} %bitcast.91), kind=kOutput, calls=%fused_computation.7 | convolution fusion | flops 268696576 | bytes 2887680 | tf_op jit(solution)/shard_map/dot_general | solution.py:215
  165.9 12.0 %psum.7 = f32[1024]{0:T(1024)S(1)} all-reduce(f32[1024]{0:T(1024)S(1)} %get-tuple-element.40), channel_id=1, replica_groups=mesh['kv_0'=8,'kv_1'=4,'tp'=8] {'tp'}, use_global_device_ids=true, to_apply=%region_6.7 | all-reduce | flops 1024 | bytes 8192 | tf_op jit(solution)/shard_map/psum | solution.py:219
  178.1 0.8 copy.159
  (71 shorter events, 4.2 us)
Async XLA Ops:
  6.5 52.9 %copy-start = (bf16[1024,256]{1,0:T(8,128)(2,1)S(1)}, bf16[1024,256]{1,0:T(8,128)(2,1)}, u32[]{:S(2)}) copy-start(bf16[1024,256]{1,0:T(8,128)(2,1)} %param.10) | copy-start | bytes 1572868
  6.5 36.0 %all-gather.3.cloned.1.call-start = ((), (), s32[]{:S(2)}) async-start(), calls=%async_computation.4 | async-start | bytes 2359296 | tf_op jit(solution)/shard_map/all_gather | solution.py:21
  47.3 10.5 %copy-start.3 = (bf16[2,128,64]{1,2,0:T(8,128)(2,1)S(1)}, bf16[2,128,64]{1,2,0:T(8,128)(2,1)}, u32[]{:S(2)}) copy-start(bf16[2,128,64]{1,2,0:T(8,128)(2,1)} %param.14) | copy-start | bytes 98308
  47.3 11.5 %copy-start.2 = (s32[8,32]{1,0:T(8,128)S(1)}, s32[8,32]{1,0:T(8,128)}, u32[]{:S(2)}) copy-start(s32[8,32]{1,0:T(8,128)} %param.17) | copy-start | bytes 3076
  47.3 58.4 %all-to-all-start.2 = ((bf16[32,2,128,128]{3,2,1,0:T(8,128)(2,1)}), bf16[32,2,128,128]{3,2,1,0:T(8,128)(2,1)S(1)}, u32[]{:S(2)}, u32[]{:S(2)}) async-start(bf16[32,2,128,128]{3,2,1,0:T(8,128)(2,1)} %broadcast_select_fusion), calls=%async_computation.2 | async-start | bytes 4194304 | tf_op jit(solution)/shard_map/all_to_all | solution.py:187
  56.9 106.6 %all-gather.5.cloned.1.call-start = ((), (), s32[]{:S(2)}) async-start(), calls=%async_computation.5 | async-start | bytes 2359296 | tf_op jit(solution)/shard_map/all_gather | solution.py:21
  107.4 27.2 %copy-start.1 = (bf16[128,1024]{1,0:T(8,128)(2,1)S(1)}, bf16[128,1024]{1,0:T(8,128)(2,1)}, u32[]{:S(2)}) copy-start(bf16[128,1024]{1,0:T(8,128)(2,1)} %param.15) | copy-start | bytes 786436
  135.4 13.1 %all-to-all-start.3 = ((bf16[128,8,128]{0,2,1:T(8,128)(2,1)}), bf16[128,8,128]{0,2,1:T(8,128)(2,1)S(1)}, u32[]{:S(2)}, u32[]{:S(2)}) async-start(bf16[128,8,128]{0,2,1:T(8,128)(2,1)} %bitcast.40), calls=%async_computation.3 | async-start | bytes 524288 | tf_op jit(solution)/shard_map/all_to_all | solution.py:211
Sparse Core Ops, SparseCore 0:
  9.2 33.3 all-gather.2
  134.7 28.7 all-gather.4

commit v2 on v1

v2 whole, which is shorter than its diff:
```python
import jax
import jax.numpy as jnp
from jax import lax
from jax.experimental import pallas as pl
from jax.experimental.pallas import tpu as pltpu
from jax.sharding import PartitionSpec as P

BLOCK = 128
PER_OWNER = 2
MESH = pl.DeviceIdType.MESH
GROUP = 8
LOG2E = 1.4426950408889634


epsilon = 1e-06
masked_score = -1e30


def taken_in(shard, axis, dim, absorb, carry):
    whole = jax.tree.map(lambda part: lax.all_gather(part, axis, axis=dim, tiled=True), shard)
    return absorb(carry, whole, jnp.int32(0))


def neighbours(tp):
    side = lax.rem(tp, 2)
    right = lax.rem(tp + 2, 8)
    left = lax.rem(tp + 6, 8)
    far = lax.rem(tp + 4, 8)
    return right, left, far, tp + 1 - 2 * side


class Spread:
    def __init__(self, full, first, size, send_sem, recv_sem):
        self.full, self.send_sem, self.recv_sem = full, send_sem, recv_sem
        half = size // 2
        self.ranges = ((first, half), (first + half, size - half))
        self.tp = lax.axis_index("tp")
        self.right, self.left, self.far, self.other = neighbours(self.tp)

    def copy(self, slot, part, dest, kind):
        first, size = self.ranges[part]
        piece = self.full.at[slot, pl.ds(first, size)]
        return pltpu.make_async_remote_copy(
            src_ref=piece,
            dst_ref=piece,
            send_sem=self.send_sem.at[kind],
            recv_sem=self.recv_sem.at[slot, part],
            device_id={"tp": dest},
            device_id_type=MESH,
        )

    def sends(self):
        me, right, left, far, other = self.tp, self.right, self.left, self.far, self.other
        return (
            (me, 0, right), (me, 1, left), (me, 1, right), (me, 0, left), (me, 0, other), (me, 1, other),
            (left, 0, right), (right, 1, left), (left, 0, other), (right, 1, other), (left, 1, other),
            (right, 0, other), (far, 0, other), (far, 1, other),
        )

    def start(self, *kinds):
        every = self.sends()
        for kind in kinds:
            self.copy(*every[kind], kind).start()

    def arrived(self, slot, part):
        self.copy(slot, part, self.other, 0).wait_recv()

    def own(self):
        self.start(0, 1, 2, 3, 4, 5)

    def relay_first(self):
        self.arrived(self.left, 0)
        self.start(6, 8)
        self.arrived(self.right, 1)
        self.start(7, 9)

    def relay_rest(self):
        self.arrived(self.left, 1)
        self.start(10)
        self.arrived(self.right, 0)
        self.start(11)
        self.arrived(self.far, 0)
        self.start(12)
        self.arrived(self.far, 1)
        self.start(13)

    def finish(self):
        side = 1 - 2 * lax.rem(self.tp, 2)
        for slot in (self.other, self.left + side, self.right + side, self.far + side):
            for part in (0, 1):
                self.arrived(slot, part)
        for kind, (slot, part, dest) in enumerate(self.sends()):
            self.copy(slot, part, dest, kind).wait_send()


def collect_kernel(
    chosen, tokens, latent_weight,
    full, pool, table,
    weight, rows, asked, asks, served,
    local_sem, rows_send, rows_recv, ask_send, ask_recv, serve_send, serve_recv,
    tok_send, tok_recv, here_send, here_recv, low_send, low_recv, high_send, high_recv,
):
    kv, tp = lax.axis_index("kv"), lax.axis_index("tp")
    owners = asked.shape[0]
    peers = full.shape[0]
    blocks, groups = rows.shape[1], peers
    group = rows.shape[2]

    own_tokens = pltpu.make_async_copy(tokens, full.at[tp], local_sem.at[0])
    own_tokens.start()
    own_weight = pltpu.make_async_copy(latent_weight, weight, local_sem.at[1])
    own_weight.start()

    barrier = pltpu.get_barrier_semaphore()

    def greet_tp(step, carry):
        pl.semaphore_signal(barrier, inc=1, device_id={"tp": lax.rem(tp + step, peers)}, device_id_type=MESH)
        return carry

    def greet_kv(step, carry):
        pl.semaphore_signal(barrier, inc=1, device_id={"kv": lax.rem(kv + step, owners)}, device_id_type=MESH)
        return carry

    lax.fori_loop(1, owners, greet_kv, 0)
    lax.fori_loop(1, peers, greet_tp, 0)

    tile = (blocks, 128)
    lane = lax.broadcasted_iota(jnp.int32, tile, 1)
    ids = lane * blocks + lax.broadcasted_iota(jnp.int32, tile, 0)

    def mark(b, needed):
        for c in range(chosen.shape[1]):
            needed = jnp.where(ids == chosen[b, c], 1, needed)
        return needed

    needed = lax.fori_loop(0, blocks, mark, jnp.zeros(tile, jnp.int32))
    first = jnp.full((1, 128), -1, jnp.int32)
    second = first
    for j in reversed(range(blocks)):
        hit = needed[j : j + 1, :] > 0
        second = jnp.where(hit, first, second)
        first = jnp.where(hit, j, first)
    sub = lax.broadcasted_iota(jnp.int32, tile, 0)
    listed = jnp.where(sub == 0, first, jnp.where(sub == 1, second, 0))
    table[...] = listed
    wide = listed.astype(jnp.float32)

    def write_ask(o, carry):
        asks[o] = jnp.broadcast_to(jnp.sum(jnp.where(lane == o, wide, 0.0), axis=1, keepdims=True), tile)
        return carry

    lax.fori_loop(0, owners, write_ask, 0)
    own_tokens.wait()
    pl.semaphore_wait(barrier, owners + peers - 2)

    def rows_copy(to):
        return pltpu.make_async_remote_copy(
            src_ref=full.at[tp, :, to],
            dst_ref=rows.at[tp],
            send_sem=rows_send.at[to],
            recv_sem=rows_recv.at[tp],
            device_id={"tp": to},
            device_id_type=MESH,
        )

    def rows_arrival(source):
        return pltpu.make_async_remote_copy(
            src_ref=rows.at[source],
            dst_ref=rows.at[source],
            send_sem=rows_send.at[source],
            recv_sem=rows_recv.at[source],
            device_id={"tp": source},
            device_id_type=MESH,
        )

    def ask_copy(owner, slot):
        return pltpu.make_async_remote_copy(
            src_ref=asks.at[owner],
            dst_ref=asked.at[slot],
            send_sem=ask_send.at[owner],
            recv_sem=ask_recv.at[slot],
            device_id={"kv": owner},
            device_id_type=MESH,
        )

    def serve_copy(to, slot):
        return pltpu.make_async_remote_copy(
            src_ref=served.at[to],
            dst_ref=pool.at[tp, pl.ds(blocks + slot * PER_OWNER, PER_OWNER)],
            send_sem=serve_send.at[to],
            recv_sem=serve_recv.at[slot],
            device_id={"kv": to},
            device_id_type=MESH,
        )

    def each(low, high, act):
        def step(i, carry):
            act(i)
            return carry

        lax.fori_loop(low, high, step, 0)

    each(1, peers, lambda i: rows_copy(lax.rem(tp + i, peers)).start())
    each(0, kv, lambda o: ask_copy(o, kv).start())
    flat = full.reshape(peers, blocks * groups, group, 128)
    token_spread = Spread(flat, 0, blocks * groups, tok_send, tok_recv)
    token_spread.own()

    rows[tp] = full[tp, :, tp]
    own_weight.wait()
    each(1, peers, lambda i: rows_arrival(lax.rem(tp + i, peers)).wait_recv())
    lines = blocks * group
    latent = jnp.zeros((lines, 128), jnp.float32)
    for p in range(peers):
        latent += jnp.dot(
            rows[p].reshape(lines, 128), weight[p * 128 : (p + 1) * 128, :], preferred_element_type=jnp.float32
        )
    latent = latent.astype(jnp.bfloat16).reshape(blocks, group, 128)
    pool[tp, 0:blocks] = latent
    latent = latent.astype(jnp.float32)

    def serve(r):
        ask_copy(r, r).wait_recv()
        for k in range(PER_OWNER):
            want = asked[r, k : k + 1, :]
            picked = jnp.zeros((group, 128), jnp.float32)
            for j in range(blocks):
                picked = jnp.where(want == float(j), latent[j], picked)
            served[r, k] = picked.astype(jnp.bfloat16)
        serve_copy(r, kv).start()

    each(kv + 1, owners, serve)
    half = owners * PER_OWNER // 2
    here = Spread(pool, 0, blocks, here_send, here_recv)
    low = Spread(pool, blocks, half, low_send, low_recv)
    high = Spread(pool, blocks + half, half, high_send, high_recv)
    here.own()
    token_spread.relay_first()

    each(0, jnp.minimum(kv, owners // 2), lambda o: serve_copy(o, o).wait_recv())
    low.own()
    each(owners // 2, jnp.maximum(kv, owners // 2), lambda o: serve_copy(o, o).wait_recv())
    high.own()
    token_spread.relay_rest()
    here.relay_first()
    low.relay_first()
    high.relay_first()
    here.relay_rest()
    low.relay_rest()
    high.relay_rest()
    each(1, peers, lambda i: rows_copy(lax.rem(tp + i, peers)).wait_send())
    each(0, kv, lambda o: ask_copy(o, kv).wait_send())
    each(kv + 1, owners, lambda r: serve_copy(r, kv).wait_send())
    for spread in (token_spread, here, low, high):
        spread.finish()


def collect(chosen, tokens, latent_weight):
    peers, owners = lax.axis_size("tp"), lax.axis_size("kv")
    blocks = chosen.shape[0]
    rows, width = tokens.shape
    group = BLOCK // peers
    slots = blocks + owners * PER_OWNER
    vmem = pl.BlockSpec(memory_space=pltpu.VMEM)
    dma = pltpu.SemaphoreType.DMA
    full, pool, table = pl.pallas_call(
        collect_kernel,
        out_shape=(
            jax.ShapeDtypeStruct((peers, blocks, peers, group, width), jnp.bfloat16),
            jax.ShapeDtypeStruct((peers, slots, group, 128), jnp.bfloat16),
            jax.ShapeDtypeStruct((blocks, 128), jnp.int32),
        ),
        in_specs=[
            pl.BlockSpec(memory_space=pltpu.SMEM),
            pl.BlockSpec(memory_space=pl.ANY),
            pl.BlockSpec(memory_space=pl.ANY),
        ],
        out_specs=(vmem, vmem, vmem),
        scratch_shapes=[
            pltpu.VMEM(latent_weight.shape, jnp.bfloat16),
            pltpu.VMEM((peers, blocks, group, width), jnp.bfloat16),
            pltpu.VMEM((owners, blocks, 128), jnp.float32),
            pltpu.VMEM((owners, blocks, 128), jnp.float32),
            pltpu.VMEM((owners, PER_OWNER, group, 128), jnp.bfloat16),
            dma((2,)),
            dma((peers,)), dma((peers,)),
            dma((owners,)), dma((owners,)),
            dma((owners,)), dma((owners,)),
            dma((14,)), dma((peers, 2)),
            dma((14,)), dma((peers, 2)),
            dma((14,)), dma((peers, 2)),
            dma((14,)), dma((peers, 2)),
        ],
        compiler_params=pltpu.CompilerParams(collective_id=0, has_side_effects=True),
    )(chosen, tokens.reshape(blocks, peers, group, width), latent_weight)
    return full.reshape(peers, rows, width), pool, table


def attend_block(
    chosen_ref, table_ref, tokens_ref, weight_ref, pool_ref, query_gain_ref, key_gain_ref, up_ref, out_ref, keys, values
):
    step = pl.program_id(0)
    kv = lax.axis_index("kv")
    peers, slots, group, width = pool_ref.shape
    heads = up_ref.shape[0]
    blocks, picks = chosen_ref.shape

    @pl.when(step == 0)
    def _():
        def prepare(j, carry):
            rows = pl.ds(pl.multiple_of(j * 2 * BLOCK, 2 * BLOCK), 2 * BLOCK)
            latent = jnp.concatenate(
                [pool_ref[:, 2 * j + i].reshape(BLOCK, width) for i in range(2)], axis=0
            )
            wide = latent.astype(jnp.float32)
            mean_sq = jnp.mean(wide * wide, axis=-1, keepdims=True)
            keys[rows, :] = (wide * lax.rsqrt(mean_sq + epsilon) * key_gain_ref[...]).astype(jnp.bfloat16)
            values[rows, :width] = latent
            values[rows, width:] = jnp.ones((2 * BLOCK, width), jnp.bfloat16)
            return carry

        lax.fori_loop(0, slots // 2, prepare, 0)
        keys[slots * BLOCK :, :] = jnp.zeros((BLOCK, width), jnp.bfloat16)
        values[slots * BLOCK :, :] = jnp.zeros((BLOCK, 2 * width), jnp.bfloat16)

    scale = width ** (-0.5) * LOG2E
    lines = pl.ds(pl.multiple_of(step * BLOCK, BLOCK), BLOCK)
    features = jnp.concatenate([tokens_ref[p, lines, :] for p in range(peers)], axis=1)
    projected = jnp.dot(features, weight_ref[...], preferred_element_type=jnp.float32).astype(jnp.bfloat16)
    parts = []
    for h in range(heads):
        wide = projected[:, h * width : (h + 1) * width].astype(jnp.float32)
        mean_sq = jnp.mean(wide * wide, axis=-1, keepdims=True)
        parts.append((wide * lax.rsqrt(mean_sq + epsilon) * (query_gain_ref[...] * scale)).astype(jnp.bfloat16))
    queries = jnp.concatenate(parts, axis=0)

    def rows_of(c):
        block = chosen_ref[step, c]
        held = jnp.maximum(block, 0)
        owner = lax.shift_right_logical(held, 3)
        inside = lax.bitwise_and(held, 7)
        remote = blocks + owner * PER_OWNER + jnp.where(table_ref[1, owner] == inside, 1, 0)
        slot = jnp.where(block < 0, slots, jnp.where(owner == kv, inside, remote))
        return pl.ds(pl.multiple_of(slot * BLOCK, BLOCK), BLOCK)

    def group(first, masked):
        places = [rows_of(first + i) for i in range(GROUP)]
        picked = jnp.concatenate([keys[r, :] for r in places], axis=0)
        scores = lax.dot_general(
            queries, picked, (((1,), (1,)), ((), ())), preferred_element_type=jnp.float32
        )
        if masked:
            row = lax.broadcasted_iota(jnp.int32, scores.shape, 0) % BLOCK
            col = lax.broadcasted_iota(jnp.int32, scores.shape, 1)
            scores = jnp.where((col <= row) | (col >= BLOCK), scores, masked_score)
        weights = jnp.exp2(scores).astype(jnp.bfloat16)
        held = jnp.concatenate([values[r, :] for r in places], axis=0)
        return jnp.dot(weights, held, preferred_element_type=jnp.float32)

    total = group(0, True)
    total = lax.fori_loop(1, picks // GROUP, lambda g, t: t + group(g * GROUP, False), total)
    attended = (total[:, :width] / total[:, width:]).astype(jnp.bfloat16)
    outs = [
        jnp.dot(attended[h * BLOCK : (h + 1) * BLOCK], up_ref[h], preferred_element_type=jnp.float32)
        for h in range(heads)
    ]
    out_ref[...] = jnp.concatenate(outs, axis=1).astype(jnp.bfloat16)


def attention(chosen, table, tokens, query_weight, pool, query_gain, key_gain, value_up):
    peers, rows, _ = tokens.shape
    _, slots, _, width = pool.shape
    heads, _, vdim = value_up.shape
    whole = pl.BlockSpec(memory_space=pltpu.VMEM)
    smem = pl.BlockSpec(memory_space=pltpu.SMEM)
    return pl.pallas_call(
        attend_block,
        grid=(rows // BLOCK,),
        out_shape=jax.ShapeDtypeStruct((rows, heads * vdim), jnp.bfloat16),
        in_specs=[smem, smem, whole, whole, whole, whole, whole, whole],
        out_specs=pl.BlockSpec((BLOCK, heads * vdim), lambda b: (b, 0)),
        scratch_shapes=[
            pltpu.VMEM(((slots + 1) * BLOCK, width), jnp.bfloat16),
            pltpu.VMEM(((slots + 1) * BLOCK, 2 * width), jnp.bfloat16),
        ],
    )(chosen, table, tokens, query_weight, pool, query_gain, key_gain, value_up)


def shards(
    tokens,
    query_weight,
    latent_weight,
    query_gain,
    key_gain,
    value_up,
    out_weight,
    out_gain,
    chosen,
):
    tok_rows = tokens.shape[0]
    lat_width = latent_weight.shape[1]
    full, pool, table = collect(chosen, tokens, latent_weight)
    heads_out = attention(
        chosen, table, full, query_weight, pool,
        query_gain.reshape(1, lat_width), key_gain.reshape(1, lat_width), value_up,
    )
    model_width = out_weight.shape[1]
    tp_count = lax.axis_size("tp")
    feature_rows = model_width // tp_count
    gain_part = lax.dynamic_slice_in_dim(
        out_gain, lax.axis_index("tp") * feature_rows, feature_rows, 0
    )
    column_block = lax.all_to_all(out_weight, "tp", split_axis=1, concat_axis=0, tiled=True)

    def contract(total, head_piece, offset):
        weight_rows = lax.dynamic_slice_in_dim(column_block, offset, head_piece.shape[1], 0)
        return total + jnp.dot(head_piece, weight_rows, preferred_element_type=jnp.float32)

    empty_cols = jnp.zeros((tok_rows, feature_rows), jnp.float32)
    summed = taken_in(heads_out, "tp", 1, contract, empty_cols)
    squares = lax.psum(jnp.sum(summed * summed, axis=1), "tp")
    mixed_out = (summed * lax.rsqrt(squares / model_width + epsilon)[:, None] * gain_part).astype(
        jnp.bfloat16
    )
    return mixed_out


def solution(mesh):
    in_specs = (
        P("kv", "tp"),
        P(None, "tp"),
        P(),
        P(),
        P(),
        P("tp", None, None),
        P("tp", None),
        P(),
        P("kv", None),
    )
    out_specs = P("kv", "tp")
    return jax.shard_map(
        shards, mesh=mesh, in_specs=in_specs, out_specs=out_specs, check_vma=False
    )
```

time: 187 us -> 133 us (0.71)
  waiting for transfers between devices: 69.8 us -> 25 us
  Pallas kernels: 27.2 us -> 71.6 us
  blocking collectives: 35.6 us -> 12 us
  starting transfers between devices: 16.2 us -> 3.44 us
  other arithmetic: 6.42 us -> 0.11 us
  matrix products: 7.81 us -> 2.42 us
  local copies, waits for them, and re-layouts: 9.33 us -> 4.14 us
    all_to_all x1 -> x0, waiting for transfers between devices: 43.2 us -> none  [shards(): lax.all_to_all(served, KV, split_axis=0, concat_axis=0, tiled=True)]
    pallas_call x0 -> x1, Pallas kernels: none -> 41.2 us  [collect(): pl.pallas_call(collect_kernel, out_shape=(jax.ShapeDtypeStruct((peers, bl...]
    all_to_all x2 -> x0, blocking collectives: 23.5 us -> none  [exchange_in_order(): result = lax.all_to_all(result, axes[k], k, k, tiled=True)]
    all_to_all x1 -> x0, starting transfers between devices: 9.58 us -> none  [shards(): lax.all_to_all(served, KV, split_axis=0, concat_axis=0, tiled=True)]
    dot_general x2 -> x0, matrix products: 5.39 us -> none  [the longest x1 3.09 us: project(): jnp.dot(shard_piece, query_rows, preferred_element_type=jnp.float32)]
    pallas_call x1, Pallas kernels: 27.2 us -> 30.4 us  [attention(): pl.pallas_call(attend_block, grid=(rows // BLOCK,), out_shape=jax.ShapeDt...]
    all_to_all x1, starting transfers between devices: 6.55 us -> 3.44 us  [shards(): lax.all_to_all(out_weight, 'tp', split_axis=1, concat_axis=0, tiled=True)]
    another operation x35 -> x0, local copies, waits for them, and re-layouts: 3.09 us -> none  [split_up(): return jnp.stack(jnp.split(shard, length, axis=dim))]
  transfers between devices with their start and end apart: 4 -> 2, of which waited for: 4 -> 2; matrix products, arithmetic and copies ran while one was open for 7% -> 1% of each run, Pallas kernels for 0% -> 0%
where the time goes in v2:
time: 133 us; the launch traced here: 132 us
  Pallas kernels  71.6 us (54%)
  waiting for transfers between devices  25 us (19%)
  between operations  13.4 us (10%)
  blocking collectives  12 us (9%)
  local copies, waits for them, and re-layouts  4.14 us (3%)
  starting transfers between devices  3.44 us (3%)
  matrix products  2.42 us (2%)
    pallas_call x1, Pallas kernels, collect(): pl.pallas_call(collect_kernel, out_shape=(jax.ShapeDtypeStruct((peers, bl...  41.2 us
    pallas_call x1, Pallas kernels, attention(): pl.pallas_call(attend_block, grid=(rows // BLOCK,), out_shape=jax.ShapeDt...  30.4 us
    all_gather x1, waiting for transfers between devices, taken_in(): lax.all_gather(part, axis, axis=dim, tiled=True)  19.2 us
    psum x1, blocking collectives, shards(): squares = lax.psum(jnp.sum(summed * summed, axis=1), 'tp')  12 us
    all_to_all x1, waiting for transfers between devices, shards(): lax.all_to_all(out_weight, 'tp', split_axis=1, concat_axis=0, tiled=True)  5.77 us
    all_to_all x1, starting transfers between devices, shards(): lax.all_to_all(out_weight, 'tp', split_axis=1, concat_axis=0, tiled=True)  3.44 us
  transfers between devices with their start and end apart: 2, of which 2 were waited for; matrix products, arithmetic and copies ran while one was open for 1% of the time, Pallas kernels for 0%

profile of v2, /device:TPU:1, one launch (start us, length us, event | category | flops | bytes accessed | tf_op | source)
XLA Modules:
  0.0 132.2 jit_solution(5986162730747587493)
XLA Ops:
  6.5 0.0 all-gather.2.cloned.1.call-start
  6.5 1.5 %copy.14.up_ref = bf16[2,128,64]{2,1,0:T(8,128)(2,1)} copy(bf16[2,128,64]{1,2,0:T(8,128)(2,1)} %param.14) | data formatting | bytes 65536 | tf_op args[5]
  8.0 41.2 %shard_map.91 = (bf16[8,8,8,16,128]{4,3,2,1,0:T(8,128)(2,1)}, bf16[8,72,16,128]{3,2,1,0:T(8,128)(2,1)}, s32[8,128]{1,0:T(8,128)}) custom-call(s32[8,32]{1,0:T(8,128)} %chosen_ref.1, bf16[8,8,16,128]{3,2,1,0:T(8,128)(2,1)} %bitcast.12, bf16[1024,128]{1,0:T(8,128)(2,1)} %latent_weight.1), custom_call_target="tpu_custom_call" | custom-call | tf_op jit(solution)/shard_map/pallas_call | solution.py:266
  49.2 0.0 copy-start
  49.3 30.4 %shard_map.92 = bf16[1024,128]{1,0:T(8,128)(2,1)} custom-call(s32[8,32]{1,0:T(8,128)} %chosen_ref.1, s32[8,128]{1,0:T(8,128)} %get-tuple-element.8.table_ref, bf16[8,1024,128]{2,1,0:T(8,128)(2,1)} %bitcast.9, bf16[1024,256]{1,0:T(8,128)(2,1)} %weight_ref.1, bf16[8,72,16,128]{3,2,1,0:T(8,128)(2,1)} %get-tuple-element.10.pool_ref, f32[1,128]{1,0:T(1,128)} %bitcast.13, ...), custom_call_target="tpu_custom_call" | custom-call | tf_op jit(solution)/shard_map/pallas_call | solution.py:376
  79.6 0.0 all-gather.2.cloned.1.call-update
  79.7 0.0 copy-done
  79.7 0.9 copy.15
  80.5 3.4 %all-to-all-start = ((bf16[128,8,128]{0,2,1:T(8,128)(2,1)}), bf16[128,8,128]{0,2,1:T(8,128)(2,1)S(1)}, u32[]{:S(2)}, u32[]{:S(2)}) async-start(bf16[128,8,128]{0,2,1:T(8,128)(2,1)} %bitcast.4), calls=%async_computation | async-start | bytes 524288 | tf_op jit(solution)/shard_map/all_to_all | solution.py:413
  84.0 0.8 dynamic_slice.3
  84.7 5.8 %all-to-all-done = bf16[128,8,128]{0,2,1:T(8,128)(2,1)S(1)} async-done(((bf16[128,8,128]{0,2,1:T(8,128)(2,1)}), bf16[128,8,128]{0,2,1:T(8,128)(2,1)S(1)}, u32[]{:S(2)}, u32[]{:S(2)}) %all-to-all-start) | async-done | bytes 262176 | tf_op jit(solution)/shard_map/all_to_all | solution.py:413
  90.5 0.2 copy.16
  90.7 19.2 %all-gather.2.cloned.1.call-done = bf16[1024,1024]{1,0:T(8,128)(2,1)} async-done(((bf16[1024,128]{1,0:T(8,128)(2,1)}), bf16[1024,1024]{1,0:T(8,128)(2,1)}) %all-gather.2.cloned.1.call-update) | async-done | bytes 2097168 | tf_op jit(solution)/shard_map/all_gather | solution.py:20
  109.9 2.4 %multiply_reduce_fusion = (f32[1024]{0:T(1024)S(1)}, f32[1024,128]{0,1:T(8,128)S(1)}) fusion(bf16[1024,1024]{1,0:T(8,128)(2,1)} %all-gather.2.cloned.1.call-done, bf16[1024,128]{1,0:T(8,128)(2,1)S(1)} %bitcast.11), kind=kOutput, calls=%fused_computation.1 | convolution fusion | flops 268696576 | bytes 2887680 | tf_op jit(solution)/shard_map/dot_general | solution.py:417
  112.3 12.0 %psum.7 = f32[1024]{0:T(1024)S(1)} all-reduce(f32[1024]{0:T(1024)S(1)} %get-tuple-element.11), channel_id=1, replica_groups=mesh['kv'=32,'tp'=8] {'tp'}, use_global_device_ids=true, to_apply=%region_1.0 | all-reduce | flops 1024 | bytes 8192 | tf_op jit(solution)/shard_map/psum | solution.py:421
  124.4 0.1 multiply_convert_fusion
  124.5 0.8 copy.17
  (1 shorter events, 0.0 us)
Async XLA Ops:
  6.5 103.4 %all-gather.2.cloned.1.call-start = ((), (), s32[]{:S(2)}) async-start(), calls=%async_computation.1 | async-start | bytes 2359296 | tf_op jit(solution)/shard_map/all_gather | solution.py:20
  49.2 30.4 %copy-start = (bf16[128,1024]{1,0:T(8,128)(2,1)S(1)}, bf16[128,1024]{1,0:T(8,128)(2,1)}, u32[]{:S(2)}) copy-start(bf16[128,1024]{1,0:T(8,128)(2,1)} %param.15) | copy-start | bytes 786436
  80.5 10.0 %all-to-all-start = ((bf16[128,8,128]{0,2,1:T(8,128)(2,1)}), bf16[128,8,128]{0,2,1:T(8,128)(2,1)S(1)}, u32[]{:S(2)}, u32[]{:S(2)}) async-start(bf16[128,8,128]{0,2,1:T(8,128)(2,1)} %bitcast.4), calls=%async_computation | async-start | bytes 524288 | tf_op jit(solution)/shard_map/all_to_all | solution.py:413
Sparse Core Ops, SparseCore 0:
  79.8 30.0 all-gather.1

commit v3 on v2

v3 whole, which is shorter than its diff:
```python
import jax
import jax.numpy as jnp
from jax import lax
from jax.experimental import pallas as pl
from jax.experimental.pallas import tpu as pltpu
from jax.sharding import PartitionSpec as P

BLOCK = 128
PER_OWNER = 2
MESH = pl.DeviceIdType.MESH
GROUP = 8
PIECES = 4
ONES = 16
HALF = 4
LOG2E = 1.4426950408889634


epsilon = 1e-06
masked_score = -1e30


def neighbours(tp):
    side = lax.rem(tp, 2)
    right = lax.rem(tp + 2, 8)
    left = lax.rem(tp + 6, 8)
    far = lax.rem(tp + 4, 8)
    return right, left, far, tp + 1 - 2 * side


class Spread:
    def __init__(self, full, first, size, send_sem, recv_sem):
        self.full, self.send_sem, self.recv_sem = full, send_sem, recv_sem
        half = size // 2
        self.ranges = ((first, half), (first + half, size - half))
        self.tp = lax.axis_index("tp")
        self.right, self.left, self.far, self.other = neighbours(self.tp)

    def copy(self, slot, part, dest, kind):
        first, size = self.ranges[part]
        piece = self.full.at[slot, pl.ds(first, size)]
        return pltpu.make_async_remote_copy(
            src_ref=piece,
            dst_ref=piece,
            send_sem=self.send_sem.at[kind],
            recv_sem=self.recv_sem.at[slot, part],
            device_id={"tp": dest},
            device_id_type=MESH,
        )

    def sends(self):
        me, right, left, far, other = self.tp, self.right, self.left, self.far, self.other
        return (
            (me, 0, right), (me, 1, left), (me, 1, right), (me, 0, left), (me, 0, other), (me, 1, other),
            (left, 0, right), (right, 1, left), (left, 0, other), (right, 1, other), (left, 1, other),
            (right, 0, other), (far, 0, other), (far, 1, other),
        )

    def start(self, *kinds):
        every = self.sends()
        for kind in kinds:
            self.copy(*every[kind], kind).start()

    def arrived(self, slot, part):
        self.copy(slot, part, self.other, 0).wait_recv()

    def own(self):
        self.start(0, 1, 2, 3, 4, 5)

    def relay_first(self):
        self.arrived(self.left, 0)
        self.start(6, 8)
        self.arrived(self.right, 1)
        self.start(7, 9)

    def relay_rest(self):
        self.arrived(self.left, 1)
        self.start(10)
        self.arrived(self.right, 0)
        self.start(11)
        self.arrived(self.far, 0)
        self.start(12)
        self.arrived(self.far, 1)
        self.start(13)

    def finish(self):
        side = 1 - 2 * lax.rem(self.tp, 2)
        for slot in (self.other, self.left + side, self.right + side, self.far + side):
            for part in (0, 1):
                self.arrived(slot, part)

    def drain(self):
        for kind, (slot, part, dest) in enumerate(self.sends()):
            self.copy(slot, part, dest, kind).wait_send()


def each(low, high, act):
    def step(i, carry):
        act(i)
        return carry

    lax.fori_loop(low, high, step, 0)


def remote(source, target, send_sem, recv_sem, axis, to):
    return pltpu.make_async_remote_copy(
        src_ref=source,
        dst_ref=target,
        send_sem=send_sem,
        recv_sem=recv_sem,
        device_id={axis: to},
        device_id_type=MESH,
    )


def unit(values, gain_row):
    mean_sq = jnp.mean(values * values, axis=-1, keepdims=True)
    return (values * lax.rsqrt(mean_sq + epsilon) * gain_row).astype(jnp.bfloat16)


def kernel(
    chosen, tokens, latent_weight, query_weight, out_weight, query_gain, key_gain, up, out_gain,
    out,
    full, pool, wide_weight, weight, projection, rows, asked, asks, served, listed, table,
    queries, keys, values, staged, heads, finished,
    local_sem, rows_send, rows_recv, ask_send, ask_recv, serve_send, serve_recv,
    heads_send, heads_recv, out_send, out_recv, spread_send, spread_recv,
):
    kv, tp = lax.axis_index("kv"), lax.axis_index("tp")
    owners, peers = asked.shape[0], full.shape[0]
    blocks, group, width = rows.shape[1:]
    picks = chosen.shape[1]
    slots = pool.shape[1]
    lines = blocks * group

    own_tokens = pltpu.make_async_copy(tokens, full.at[tp], local_sem.at[0])
    own_latent = pltpu.make_async_copy(latent_weight, weight, local_sem.at[1])
    own_query = pltpu.make_async_copy(query_weight, projection, local_sem.at[2])
    own_out = pltpu.make_async_copy(out_weight, wide_weight.at[tp], local_sem.at[3])
    for copy in (own_tokens, own_latent, own_query, own_out):
        copy.start()

    barrier = pltpu.get_barrier_semaphore()

    def greet(axis, index, size):
        def signal(step):
            pl.semaphore_signal(barrier, inc=1, device_id={axis: lax.rem(index + step, size)}, device_id_type=MESH)

        each(1, size, signal)

    greet("kv", kv, owners)
    greet("tp", tp, peers)

    tile = (blocks, 128)
    lane = lax.broadcasted_iota(jnp.int32, tile, 1)
    sub = lax.broadcasted_iota(jnp.int32, tile, 0)
    ids = lane * blocks + sub

    def mark(b, needed):
        for c in range(picks):
            needed = jnp.where(ids == chosen[b, c], 1, needed)
        return needed

    needed = lax.fori_loop(0, blocks, mark, jnp.zeros(tile, jnp.int32))
    first = jnp.full((1, 128), -1, jnp.int32)
    second = first
    for j in reversed(range(blocks)):
        hit = needed[j : j + 1, :] > 0
        second = jnp.where(hit, first, second)
        first = jnp.where(hit, j, first)
    both = jnp.where(sub == 0, first, jnp.where(sub == 1, second, 0))
    listed[...] = both
    to_scalars = pltpu.make_async_copy(listed, table, local_sem.at[4])
    to_scalars.start()
    both = both.astype(jnp.float32)

    def write_ask(o):
        asks[o] = jnp.broadcast_to(jnp.sum(jnp.where(lane == o, both, 0.0), axis=1, keepdims=True), tile)

    each(0, owners, write_ask)
    own_tokens.wait()
    pl.semaphore_wait(barrier, owners + peers - 2)

    def rows_copy(to, slot):
        return remote(full.at[tp, :, to], rows.at[slot], rows_send.at[to], rows_recv.at[slot], "tp", to)

    def ask_copy(to, slot):
        return remote(asks.at[to], asked.at[slot], ask_send.at[to], ask_recv.at[slot], "kv", to)

    def serve_copy(to, slot):
        target = pool.at[tp, pl.ds(blocks + slot * PER_OWNER, PER_OWNER)]
        return remote(served.at[to], target, serve_send.at[to], serve_recv.at[slot], "kv", to)

    def peer(i):
        return lax.rem(tp + i, peers)

    each(1, peers, lambda i: rows_copy(peer(i), tp).start())
    each(0, kv, lambda o: ask_copy(o, kv).start())
    token_spread = Spread(
        full.reshape(peers, blocks * peers, group, width), 0, blocks * peers, spread_send.at[0], spread_recv.at[0]
    )
    token_spread.own()

    rows[tp] = full[tp, :, tp]
    own_latent.wait()
    each(1, peers, lambda i: rows_copy(peer(i), peer(i)).wait_recv())
    features = jnp.concatenate([rows[p].reshape(lines, width) for p in range(peers)], axis=1)
    latent = jnp.dot(features, weight[...], preferred_element_type=jnp.float32)
    latent = latent.astype(jnp.bfloat16).reshape(blocks, group, 128)
    pool[tp, 0:blocks] = latent
    latent = latent.astype(jnp.float32)

    def serve(i):
        r = owners - 1 - i
        ask_copy(r, r).wait_recv()
        for k in range(PER_OWNER):
            want = asked[r, k : k + 1, :]
            picked = jnp.zeros((group, 128), jnp.float32)
            for j in range(blocks):
                picked = jnp.where(want == float(j), latent[j], picked)
            served[r, k] = picked.astype(jnp.bfloat16)
        serve_copy(r, kv).start()

    each(0, owners - 1 - kv, serve)
    here = Spread(pool, 0, blocks, spread_send.at[1], spread_recv.at[1])
    here.own()

    share = owners // PIECES
    spreads = [
        Spread(pool, blocks + i * share * PER_OWNER, share * PER_OWNER, spread_send.at[2 + i], spread_recv.at[2 + i])
        for i in range(PIECES)
    ]

    def gathered(i):
        low = i * share
        each(low, jnp.clip(kv, low, low + share), lambda o: serve_copy(o, o).wait_recv())
        spreads[i].own()

    scale = width ** (-0.5) * LOG2E
    query_row = query_gain[...] * scale

    def project(b):
        features = jnp.concatenate([full[p, b].reshape(BLOCK, width) for p in range(peers)], axis=1)
        projected = jnp.dot(features, projection[...], preferred_element_type=jnp.float32)
        projected = projected.astype(jnp.bfloat16).astype(jnp.float32)
        for h in range(up.shape[0]):
            queries[b, h * BLOCK : (h + 1) * BLOCK, :] = unit(projected[:, h * 128 : (h + 1) * 128], query_row)

    def prepare(low, high):
        def pair(j):
            for i in range(2):
                slot = low + 2 * j + i
                block = pool[:, slot].reshape(BLOCK, width).astype(jnp.float32)
                keys[slot] = unit(block, key_gain[...])
                values[slot, :BLOCK, :] = jnp.transpose(block).astype(jnp.bfloat16)

        each(0, (high - low) // 2, pair)

    token_spread.relay_first()
    gathered(0)
    token_spread.relay_rest()
    here.relay_first()
    gathered(1)
    here.relay_rest()
    token_spread.finish()
    own_query.wait()
    each(0, blocks // 2, project)
    spreads[0].relay_first()
    gathered(2)
    spreads[1].relay_first()
    gathered(3)
    spreads[2].relay_first()
    spreads[0].relay_rest()
    spreads[3].relay_first()
    for i in range(1, PIECES):
        spreads[i].relay_rest()
    own_out.wait()
    out_spread = Spread(wide_weight, 0, 128, spread_send.at[2 + PIECES], spread_recv.at[2 + PIECES])
    out_spread.own()
    each(blocks // 2, blocks, project)
    ones = jnp.ones((ONES, BLOCK), jnp.bfloat16)

    def fill(slot):
        values[slot, BLOCK:, :] = ones

    each(0, slots, fill)
    keys[slots] = jnp.zeros((BLOCK, width), jnp.bfloat16)
    values[slots] = jnp.zeros((BLOCK + ONES, BLOCK), jnp.bfloat16)
    here.finish()
    prepare(0, blocks)
    for i in range(PIECES):
        spreads[i].finish()
        prepare(blocks + i * share * PER_OWNER, blocks + (i + 1) * share * PER_OWNER)
    to_scalars.wait()

    def heads_copy(to, b, slot):
        return remote(staged.at[b, to], heads.at[slot, b], heads_send.at[to, b], heads_recv.at[slot, b], "tp", to)

    def attend(b):
        def slot_of(c):
            block = chosen[b, c]
            held = jnp.maximum(block, 0)
            owner = lax.div(held, blocks)
            inside = held - owner * blocks
            away = blocks + owner * PER_OWNER + jnp.where(table[1, owner] == inside, 1, 0)
            return jnp.where(block < 0, slots, jnp.where(owner == kv, inside, away))

        def grouped(start, masked):
            places = [slot_of(start + i) for i in range(GROUP)]
            picked = jnp.concatenate([keys[s] for s in places], axis=0)
            scores = lax.dot_general(
                picked, queries[b], (((1,), (1,)), ((), ())), preferred_element_type=jnp.float32
            )
            if masked:
                key = lax.broadcasted_iota(jnp.int32, (BLOCK, scores.shape[1]), 0)
                query = lax.rem(lax.broadcasted_iota(jnp.int32, (BLOCK, scores.shape[1]), 1), BLOCK)
                diagonal = jnp.where(key <= query, scores[:BLOCK], masked_score)
                scores = jnp.concatenate([diagonal, scores[BLOCK:]], axis=0)
            weights = jnp.exp2(scores).astype(jnp.bfloat16)
            held = jnp.concatenate([values[s] for s in places], axis=1)
            return jnp.dot(held, weights, preferred_element_type=jnp.float32)

        total = grouped(0, True)
        total = lax.fori_loop(1, picks // GROUP, lambda g, t: t + grouped(g * GROUP, False), total)
        attended = (total[:BLOCK] / total[BLOCK : BLOCK + 1]).astype(jnp.bfloat16)
        turned = jnp.concatenate(
            [
                jnp.dot(up[h], attended[:, h * BLOCK : (h + 1) * BLOCK], preferred_element_type=jnp.float32)
                for h in range(up.shape[0])
            ],
            axis=0,
        )
        staged[b] = jnp.transpose(turned).astype(jnp.bfloat16).reshape(peers, group, width)
        each(1, peers, lambda i: heads_copy(peer(i), b, tp).start())

    def out_copy(to, half, slot):
        lower = pl.ds(half * HALF, HALF)
        return remote(
            finished.at[to, lower], out.at[lower, slot], out_send.at[to, half], out_recv.at[slot, half], "tp", to
        )

    def conclude(half):
        lower = pl.ds(half * HALF, HALF)

        def landed(i):
            for b in range(HALF):
                heads_copy(peer(i), half * HALF + b, peer(i)).wait_recv()

        each(1, peers, landed)
        for b in range(HALF):
            heads[tp, half * HALF + b] = staged[half * HALF + b, tp]
        features = jnp.concatenate([heads[p, lower].reshape(HALF * group, width) for p in range(peers)], axis=1)
        summed = jnp.dot(
            features, wide_weight[...].reshape(peers * 128, peers * 128), preferred_element_type=jnp.float32
        )
        mixed = unit(summed, out_gain[...])
        for t in range(peers):
            finished[t, lower] = mixed[:, t * 128 : (t + 1) * 128].reshape(HALF, group, 128)
        each(1, peers, lambda i: out_copy(peer(i), half, tp).start())
        out[lower, tp] = finished[tp, lower]

    def turn(b):
        attend(b)

        @pl.when(b == 1)
        def _():
            out_spread.relay_first()

        @pl.when(b == 3)
        def _():
            out_spread.relay_rest()

        @pl.when(b == 5)
        def _():
            out_spread.finish()
            conclude(0)

    each(0, blocks, turn)
    conclude(1)

    each(1, peers, lambda i: rows_copy(peer(i), tp).wait_send())
    each(0, kv, lambda o: ask_copy(o, kv).wait_send())
    each(kv + 1, owners, lambda r: serve_copy(r, kv).wait_send())
    for spread in (token_spread, here, out_spread, *spreads):
        spread.drain()

    def settle(i):
        for b in range(blocks):
            heads_copy(peer(i), b, tp).wait_send()
        for half in range(2):
            out_copy(peer(i), half, tp).wait_send()
            out_copy(peer(i), half, peer(i)).wait_recv()

    each(1, peers, settle)


def shards(
    tokens, query_weight, latent_weight, query_gain, key_gain, value_up, out_weight, out_gain, chosen
):
    peers, owners = lax.axis_size("tp"), lax.axis_size("kv")
    blocks, picks = chosen.shape
    rows, width = tokens.shape
    group = BLOCK // peers
    slots = blocks + owners * PER_OWNER
    heads = value_up.shape[0]
    vmem = pl.BlockSpec(memory_space=pltpu.VMEM)
    anywhere = pl.BlockSpec(memory_space=pl.ANY)
    dma = pltpu.SemaphoreType.DMA
    bf16 = jnp.bfloat16
    mixed = pl.pallas_call(
        kernel,
        out_shape=jax.ShapeDtypeStruct((blocks, peers, group, width), bf16),
        in_specs=[pl.BlockSpec(memory_space=pltpu.SMEM)] + [anywhere] * 4 + [vmem] * 4,
        out_specs=vmem,
        scratch_shapes=[
            pltpu.VMEM((peers, blocks, peers, group, width), bf16),
            pltpu.VMEM((peers, slots, group, width), bf16),
            pltpu.VMEM((peers, *out_weight.shape), bf16),
            pltpu.VMEM(latent_weight.shape, bf16),
            pltpu.VMEM(query_weight.shape, bf16),
            pltpu.VMEM((peers, blocks, group, width), bf16),
            pltpu.VMEM((owners, blocks, 128), jnp.float32),
            pltpu.VMEM((owners, blocks, 128), jnp.float32),
            pltpu.VMEM((owners, PER_OWNER, group, width), bf16),
            pltpu.VMEM((blocks, 128), jnp.int32),
            pltpu.SMEM((blocks, 128), jnp.int32),
            pltpu.VMEM((blocks, heads * BLOCK, width), bf16),
            pltpu.VMEM((slots + 1, BLOCK, width), bf16),
            pltpu.VMEM((slots + 1, BLOCK + ONES, BLOCK), bf16),
            pltpu.VMEM((blocks, peers, group, width), bf16),
            pltpu.VMEM((peers, blocks, group, width), bf16),
            pltpu.VMEM((peers, blocks, group, width), bf16),
            dma((5,)),
            dma((peers,)), dma((peers,)),
            dma((owners,)), dma((owners,)),
            dma((owners,)), dma((owners,)),
            dma((peers, blocks)), dma((peers, blocks)),
            dma((peers, 2)), dma((peers, 2)),
            dma((3 + PIECES, 14)), dma((3 + PIECES, peers, 2)),
        ],
        compiler_params=pltpu.CompilerParams(collective_id=0, has_side_effects=True),
    )(
        chosen,
        tokens.reshape(blocks, peers, group, width),
        latent_weight,
        query_weight,
        out_weight,
        query_gain.reshape(1, width),
        key_gain.reshape(1, width),
        jnp.swapaxes(value_up, 1, 2),
        out_gain.reshape(1, out_gain.shape[0]),
    )
    return mixed.reshape(rows, width)


def solution(mesh):
    in_specs = (
        P("kv", "tp"),
        P(None, "tp"),
        P(),
        P(),
        P(),
        P("tp", None, None),
        P("tp", None),
        P(),
        P("kv", None),
    )
    return jax.shard_map(shards, mesh=mesh, in_specs=in_specs, out_specs=P("kv", "tp"), check_vma=False)
```

time: 133 us -> 85.1 us (0.64)
  waiting for transfers between devices: 25 us -> 0 us
  between operations: 13.4 us -> 0.01 us
  blocking collectives: 12 us -> 0 us
  Pallas kernels: 71.6 us -> 83.3 us
  starting transfers between devices: 3.44 us -> 0 us
  local copies, waits for them, and re-layouts: 4.14 us -> 1.67 us
  matrix products: 2.42 us -> 0 us
    all_gather x1 -> x0, waiting for transfers between devices: 19.2 us -> none  [taken_in(): lax.all_gather(part, axis, axis=dim, tiled=True)]
    psum x1 -> x0, blocking collectives: 12 us -> none  [shards(): squares = lax.psum(jnp.sum(summed * summed, axis=1), 'tp')]
    pallas_call x2 -> x1, Pallas kernels: 71.6 us -> 83.3 us  [shards(): pl.pallas_call(kernel, out_shape=jax.ShapeDtypeStruct((blocks, peers, gro...]
    all_to_all x1 -> x0, waiting for transfers between devices: 5.77 us -> none  [shards(): lax.all_to_all(out_weight, 'tp', split_axis=1, concat_axis=0, tiled=True)]
    all_to_all x1 -> x0, starting transfers between devices: 3.44 us -> none  [shards(): lax.all_to_all(out_weight, 'tp', split_axis=1, concat_axis=0, tiled=True)]
    dot_general x1 -> x0, matrix products: 2.42 us -> none  [contract(): jnp.dot(head_piece, weight_rows, preferred_element_type=jnp.float32)]
  transfers between devices with their start and end apart: 2 -> 0, of which waited for: 2 -> 0; matrix products, arithmetic and copies ran while one was open for 1% -> 0% of each run, Pallas kernels for 0% -> 0%
where the time goes in v3:
time: 85.1 us; the launch traced here: 85 us
  Pallas kernels  83.3 us (98%)
  local copies, waits for them, and re-layouts  1.67 us (2%)
    pallas_call x1, Pallas kernels, shards(): pl.pallas_call(kernel, out_shape=jax.ShapeDtypeStruct((blocks, peers, gro...  83.3 us

profile of v3, /device:TPU:1, one launch (start us, length us, event | category | flops | bytes accessed | tf_op | source)
XLA Modules:
  0.0 85.0 jit_solution(12040489923550262478)
XLA Ops:
  0.0 83.3 %shard_map.91 = bf16[8,8,16,128]{3,2,1,0:T(8,128)(2,1)} custom-call(s32[8,32]{1,0:T(8,128)} %chosen.1, bf16[8,8,16,128]{3,2,1,0:T(8,128)(2,1)} %bitcast.7, bf16[1024,128]{1,0:T(8,128)(2,1)} %latent_weight.1, bf16[1024,256]{1,0:T(8,128)(2,1)} %query_weight.1, bf16[128,1024]{1,0:T(8,128)(2,1)} %out_weight.1, f32[1,128]{1,0:T(1,128)} %bitcast.10, ...), custom_call_target="tpu_custom_call" | custom-call | tf_op jit(solution)/shard_map/pallas_call | solution.py:409
  83.3 1.7 %copy.11 = bf16[1024,128]{1,0:T(8,128)(2,1)} copy(bf16[1024,128]{1,0:T(8,128)(2,1)} %bitcast.6) | data formatting | bytes 524288

commit v4 on v3

--- a/solution.py
+++ b/solution.py
@@ -1,3 +1,5 @@
+import functools
+
 import jax
 import jax.numpy as jnp
 from jax import lax
@@ -121,7 +123,7 @@
     chosen, tokens, latent_weight, query_weight, out_weight, query_gain, key_gain, up, out_gain,
     out,
     full, pool, wide_weight, weight, projection, rows, asked, asks, served, listed, table,
-    queries, keys, values, staged, heads, finished,
+    queries, keys, values, places, staged, heads,
     local_sem, rows_send, rows_recv, ask_send, ask_recv, serve_send, serve_recv,
     heads_send, heads_recv, out_send, out_recv, spread_send, spread_recv,
 ):
@@ -149,6 +151,28 @@
 
     greet("kv", kv, owners)
     greet("tp", tp, peers)
+
+    own_tokens.wait()
+    pl.semaphore_wait(barrier, owners + peers - 2)
+
+    def rows_copy(to, slot):
+        return remote(full.at[tp, :, to], rows.at[slot], rows_send.at[to], rows_recv.at[slot], "tp", to)
+
+    def ask_copy(to, slot):
+        return remote(asks.at[to], asked.at[slot], ask_send.at[to], ask_recv.at[slot], "kv", to)
+
+    def serve_copy(to, slot):
+        target = pool.at[tp, pl.ds(blocks + slot * PER_OWNER, PER_OWNER)]
+        return remote(served.at[to], target, serve_send.at[to], serve_recv.at[slot], "kv", to)
+
+    def peer(i):
+        return lax.rem(tp + i, peers)
+
+    each(1, peers, lambda i: rows_copy(peer(i), tp).start())
+    token_spread = Spread(
+        full.reshape(peers, blocks * peers, group, width), 0, blocks * peers, spread_send.at[0], spread_recv.at[0]
+    )
+    token_spread.own()
 
     tile = (blocks, 128)
     lane = lax.broadcasted_iota(jnp.int32, tile, 1)
@@ -173,39 +197,28 @@
     to_scalars.start()
     both = both.astype(jnp.float32)
 
-    def write_ask(o):
+    for o in range(owners - 1):
         asks[o] = jnp.broadcast_to(jnp.sum(jnp.where(lane == o, both, 0.0), axis=1, keepdims=True), tile)
-
-    each(0, owners, write_ask)
-    own_tokens.wait()
-    pl.semaphore_wait(barrier, owners + peers - 2)
-
-    def rows_copy(to, slot):
-        return remote(full.at[tp, :, to], rows.at[slot], rows_send.at[to], rows_recv.at[slot], "tp", to)
-
-    def ask_copy(to, slot):
-        return remote(asks.at[to], asked.at[slot], ask_send.at[to], ask_recv.at[slot], "kv", to)
-
-    def serve_copy(to, slot):
-        target = pool.at[tp, pl.ds(blocks + slot * PER_OWNER, PER_OWNER)]
-        return remote(served.at[to], target, serve_send.at[to], serve_recv.at[slot], "kv", to)
-
-    def peer(i):
-        return lax.rem(tp + i, peers)
-
-    each(1, peers, lambda i: rows_copy(peer(i), tp).start())
     each(0, kv, lambda o: ask_copy(o, kv).start())
-    token_spread = Spread(
-        full.reshape(peers, blocks * peers, group, width), 0, blocks * peers, spread_send.at[0], spread_recv.at[0]
-    )
-    token_spread.own()
-
+
+    ones = jnp.ones((ONES, BLOCK), jnp.bfloat16)
+
+    def fill(slot):
+        values[slot, BLOCK:, :] = ones
+
+    each(0, slots, fill)
+    keys[slots] = jnp.zeros((BLOCK, width), jnp.bfloat16)
+    values[slots] = jnp.zeros((BLOCK + ONES, BLOCK), jnp.bfloat16)
     rows[tp] = full[tp, :, tp]
     own_latent.wait()
     each(1, peers, lambda i: rows_copy(peer(i), peer(i)).wait_recv())
-    features = jnp.concatenate([rows[p].reshape(lines, width) for p in range(peers)], axis=1)
-    latent = jnp.dot(features, weight[...], preferred_element_type=jnp.float32)
-    latent = latent.astype(jnp.bfloat16).reshape(blocks, group, 128)
+    @jax.jit
+    def compress():
+        features = jnp.concatenate([rows[p].reshape(lines, width) for p in range(peers)], axis=1)
+        latent = jnp.dot(features, weight[...], preferred_element_type=jnp.float32)
+        return latent.astype(jnp.bfloat16).reshape(blocks, group, 128)
+
+    latent = compress()
     pool[tp, 0:blocks] = latent
     latent = latent.astype(jnp.float32)
 
@@ -246,67 +259,59 @@
             queries[b, h * BLOCK : (h + 1) * BLOCK, :] = unit(projected[:, h * 128 : (h + 1) * 128], query_row)
 
     def prepare(low, high):
-        def pair(j):
-            for i in range(2):
-                slot = low + 2 * j + i
+        def several(j):
+            for i in range(4):
+                slot = low + 4 * j + i
                 block = pool[:, slot].reshape(BLOCK, width).astype(jnp.float32)
                 keys[slot] = unit(block, key_gain[...])
                 values[slot, :BLOCK, :] = jnp.transpose(block).astype(jnp.bfloat16)
 
-        each(0, (high - low) // 2, pair)
-
-    token_spread.relay_first()
-    gathered(0)
-    token_spread.relay_rest()
-    here.relay_first()
-    gathered(1)
-    here.relay_rest()
-    token_spread.finish()
-    own_query.wait()
-    each(0, blocks // 2, project)
-    spreads[0].relay_first()
-    gathered(2)
-    spreads[1].relay_first()
-    gathered(3)
-    spreads[2].relay_first()
-    spreads[0].relay_rest()
-    spreads[3].relay_first()
-    for i in range(1, PIECES):
-        spreads[i].relay_rest()
-    own_out.wait()
-    out_spread = Spread(wide_weight, 0, 128, spread_send.at[2 + PIECES], spread_recv.at[2 + PIECES])
-    out_spread.own()
-    each(blocks // 2, blocks, project)
-    ones = jnp.ones((ONES, BLOCK), jnp.bfloat16)
-
-    def fill(slot):
-        values[slot, BLOCK:, :] = ones
-
-    each(0, slots, fill)
-    keys[slots] = jnp.zeros((BLOCK, width), jnp.bfloat16)
-    values[slots] = jnp.zeros((BLOCK + ONES, BLOCK), jnp.bfloat16)
-    here.finish()
-    prepare(0, blocks)
-    for i in range(PIECES):
-        spreads[i].finish()
-        prepare(blocks + i * share * PER_OWNER, blocks + (i + 1) * share * PER_OWNER)
-    to_scalars.wait()
-
-    def heads_copy(to, b, slot):
-        return remote(staged.at[b, to], heads.at[slot, b], heads_send.at[to, b], heads_recv.at[slot, b], "tp", to)
-
-    def attend(b):
-        def slot_of(c):
+        each(0, (high - low) // 4, several)
+
+    def place(b):
+        for c in range(picks):
             block = chosen[b, c]
             held = jnp.maximum(block, 0)
             owner = lax.div(held, blocks)
             inside = held - owner * blocks
             away = blocks + owner * PER_OWNER + jnp.where(table[1, owner] == inside, 1, 0)
-            return jnp.where(block < 0, slots, jnp.where(owner == kv, inside, away))
-
+            places[b, c] = jnp.where(block < 0, slots, jnp.where(owner == kv, inside, away))
+
+    to_scalars.wait()
+    each(1, peers, lambda i: rows_copy(peer(i), tp).wait_send())
+    each(0, blocks, place)
+    own_query.wait()
+    own_out.wait()
+    token_spread.relay_first()
+    here.relay_first()
+    for i in range(PIECES):
+        gathered(i)
+    here.relay_rest()
+    token_spread.relay_rest()
+    token_spread.finish()
+    token_spread.drain()
+    here.finish()
+    step = blocks // PIECES
+    for i in range(PIECES):
+        spreads[i].relay_first()
+        each(i * step, (i + 1) * step, project)
+        if i == 0:
+            prepare(0, blocks)
+    out_spread = Spread(wide_weight, 0, 128, spread_send.at[2 + PIECES], spread_recv.at[2 + PIECES])
+    for i in range(PIECES):
+        spreads[i].relay_rest()
+        if i == PIECES - 1:
+            out_spread.own()
+        spreads[i].finish()
+        prepare(blocks + i * share * PER_OWNER, blocks + (i + 1) * share * PER_OWNER)
+
+    def heads_copy(to, b, slot):
+        return remote(staged.at[b, to], heads.at[slot, b], heads_send.at[to, b], heads_recv.at[slot, b], "tp", to)
+
+    def attend(b):
         def grouped(start, masked):
-            places = [slot_of(start + i) for i in range(GROUP)]
-            picked = jnp.concatenate([keys[s] for s in places], axis=0)
+            chose = [places[b, start + i] for i in range(GROUP)]
+            picked = jnp.concatenate([keys[s] for s in chose], axis=0)
             scores = lax.dot_general(
                 picked, queries[b], (((1,), (1,)), ((), ())), preferred_element_type=jnp.float32
             )
@@ -316,7 +321,7 @@
                 diagonal = jnp.where(key <= query, scores[:BLOCK], masked_score)
                 scores = jnp.concatenate([diagonal, scores[BLOCK:]], axis=0)
             weights = jnp.exp2(scores).astype(jnp.bfloat16)
-            held = jnp.concatenate([values[s] for s in places], axis=1)
+            held = jnp.concatenate([values[s] for s in chose], axis=1)
             return jnp.dot(held, weights, preferred_element_type=jnp.float32)
 
         total = grouped(0, True)
@@ -335,52 +340,53 @@
     def out_copy(to, half, slot):
         lower = pl.ds(half * HALF, HALF)
         return remote(
-            finished.at[to, lower], out.at[lower, slot], out_send.at[to, half], out_recv.at[slot, half], "tp", to
+            rows.at[to, lower], out.at[lower, slot], out_send.at[to, half], out_recv.at[slot, half], "tp", to
         )
 
-    def conclude(half):
+    @functools.partial(jax.jit, static_argnums=0)
+    def mix(half):
         lower = pl.ds(half * HALF, HALF)
-
-        def landed(i):
-            for b in range(HALF):
-                heads_copy(peer(i), half * HALF + b, peer(i)).wait_recv()
-
-        each(1, peers, landed)
-        for b in range(HALF):
-            heads[tp, half * HALF + b] = staged[half * HALF + b, tp]
         features = jnp.concatenate([heads[p, lower].reshape(HALF * group, width) for p in range(peers)], axis=1)
         summed = jnp.dot(
             features, wide_weight[...].reshape(peers * 128, peers * 128), preferred_element_type=jnp.float32
         )
         mixed = unit(summed, out_gain[...])
         for t in range(peers):
-            finished[t, lower] = mixed[:, t * 128 : (t + 1) * 128].reshape(HALF, group, 128)
+            rows[t, lower] = mixed[:, t * 128 : (t + 1) * 128].reshape(HALF, group, 128)
+
+    def conclude(half):
+        lower = pl.ds(half * HALF, HALF)
+
+        def landed(i):
+            for b in range(HALF):
+                heads_copy(peer(i), half * HALF + b, peer(i)).wait_recv()
+
+        each(1, peers, landed)
+        for b in range(HALF):
+            heads[tp, half * HALF + b] = staged[half * HALF + b, tp]
+        mix(half)
         each(1, peers, lambda i: out_copy(peer(i), half, tp).start())
-        out[lower, tp] = finished[tp, lower]
-
-    def turn(b):
-        attend(b)
-
-        @pl.when(b == 1)
+        out[lower, tp] = rows[tp, lower]
+
+    def turn(i):
+        attend(i)
+
+        @pl.when(i == 2)
         def _():
             out_spread.relay_first()
 
-        @pl.when(b == 3)
+        @pl.when(i == 4)
         def _():
             out_spread.relay_rest()
 
-        @pl.when(b == 5)
-        def _():
-            out_spread.finish()
-            conclude(0)
-
     each(0, blocks, turn)
+    out_spread.finish()
+    conclude(0)
     conclude(1)
 
-    each(1, peers, lambda i: rows_copy(peer(i), tp).wait_send())
     each(0, kv, lambda o: ask_copy(o, kv).wait_send())
     each(kv + 1, owners, lambda r: serve_copy(r, kv).wait_send())
-    for spread in (token_spread, here, out_spread, *spreads):
+    for spread in (here, out_spread, *spreads):
         spread.drain()
 
     def settle(i):
@@ -426,8 +432,8 @@
             pltpu.VMEM((blocks, heads * BLOCK, width), bf16),
             pltpu.VMEM((slots + 1, BLOCK, width), bf16),
             pltpu.VMEM((slots + 1, BLOCK + ONES, BLOCK), bf16),
+            pltpu.SMEM((blocks, picks), jnp.int32),
             pltpu.VMEM((blocks, peers, group, width), bf16),
-            pltpu.VMEM((peers, blocks, group, width), bf16),
             pltpu.VMEM((peers, blocks, group, width), bf16),
             dma((5,)),
             dma((peers,)), dma((peers,)),

time: 85.1 us -> 78.3 us (0.920)
  Pallas kernels: 83.3 us -> 76.5 us
    pallas_call x1, Pallas kernels: 83.3 us -> 76.5 us  [shards(): pl.pallas_call(kernel, out_shape=jax.ShapeDtypeStruct((blocks, peers, gro...]
where the time goes in v4:
time: 78.3 us; the launch traced here: 78.1 us
  Pallas kernels  76.5 us (98%)
  local copies, waits for them, and re-layouts  1.67 us (2%)
    pallas_call x1, Pallas kernels, shards(): pl.pallas_call(kernel, out_shape=jax.ShapeDtypeStruct((blocks, peers, gro...  76.5 us
    unnamed x1, local copies, waits for them, and re-layouts  1.67 us

profile of v4, /device:TPU:1, one launch (start us, length us, event | category | flops | bytes accessed | tf_op | source)
XLA Modules:
  0.0 78.1 jit_solution(5352132174428261672)
XLA Ops:
  0.0 76.5 %shard_map.91 = bf16[8,8,16,128]{3,2,1,0:T(8,128)(2,1)} custom-call(s32[8,32]{1,0:T(8,128)} %chosen.1, bf16[8,8,16,128]{3,2,1,0:T(8,128)(2,1)} %bitcast.7, bf16[1024,128]{1,0:T(8,128)(2,1)} %latent_weight.1, bf16[1024,256]{1,0:T(8,128)(2,1)} %query_weight.1, bf16[128,1024]{1,0:T(8,128)(2,1)} %out_weight.1, f32[1,128]{1,0:T(1,128)} %bitcast.10, ...), custom_call_target="tpu_custom_call" | custom-call | tf_op jit(solution)/shard_map/pallas_call | solution.py:415
  76.5 1.7 %copy.11 = bf16[1024,128]{1,0:T(8,128)(2,1)} copy(bf16[1024,128]{1,0:T(8,128)(2,1)} %bitcast.6) | data formatting | bytes 524288

commit v5 on v4

--- a/solution.py
+++ b/solution.py
@@ -123,7 +123,7 @@
     chosen, tokens, latent_weight, query_weight, out_weight, query_gain, key_gain, up, out_gain,
     out,
     full, pool, wide_weight, weight, projection, rows, asked, asks, served, listed, table,
-    queries, keys, values, places, staged, heads,
+    queries, keys, values, totals, bias, places, staged, heads,
     local_sem, rows_send, rows_recv, ask_send, ask_recv, serve_send, serve_recv,
     heads_send, heads_recv, out_send, out_recv, spread_send, spread_recv,
 ):
@@ -207,6 +207,10 @@
         values[slot, BLOCK:, :] = ones
 
     each(0, slots, fill)
+    key = lax.broadcasted_iota(jnp.int32, bias.shape[1:], 0)
+    query = lax.rem(lax.broadcasted_iota(jnp.int32, bias.shape[1:], 1), BLOCK)
+    bias[0] = jnp.where(key <= query, 0.0, masked_score)
+    bias[1] = jnp.zeros(bias.shape[1:], jnp.float32)
     keys[slots] = jnp.zeros((BLOCK, width), jnp.bfloat16)
     values[slots] = jnp.zeros((BLOCK + ONES, BLOCK), jnp.bfloat16)
     rows[tp] = full[tp, :, tp]
@@ -308,34 +312,59 @@
     def heads_copy(to, b, slot):
         return remote(staged.at[b, to], heads.at[slot, b], heads_send.at[to, b], heads_recv.at[slot, b], "tp", to)
 
-    def attend(b):
-        def grouped(start, masked):
-            chose = [places[b, start + i] for i in range(GROUP)]
-            picked = jnp.concatenate([keys[s] for s in chose], axis=0)
-            scores = lax.dot_general(
-                picked, queries[b], (((1,), (1,)), ((), ())), preferred_element_type=jnp.float32
-            )
-            if masked:
-                key = lax.broadcasted_iota(jnp.int32, (BLOCK, scores.shape[1]), 0)
-                query = lax.rem(lax.broadcasted_iota(jnp.int32, (BLOCK, scores.shape[1]), 1), BLOCK)
-                diagonal = jnp.where(key <= query, scores[:BLOCK], masked_score)
-                scores = jnp.concatenate([diagonal, scores[BLOCK:]], axis=0)
-            weights = jnp.exp2(scores).astype(jnp.bfloat16)
-            held = jnp.concatenate([values[s] for s in chose], axis=1)
-            return jnp.dot(held, weights, preferred_element_type=jnp.float32)
-
-        total = grouped(0, True)
-        total = lax.fori_loop(1, picks // GROUP, lambda g, t: t + grouped(g * GROUP, False), total)
-        attended = (total[:BLOCK] / total[BLOCK : BLOCK + 1]).astype(jnp.bfloat16)
-        turned = jnp.concatenate(
-            [
-                jnp.dot(up[h], attended[:, h * BLOCK : (h + 1) * BLOCK], preferred_element_type=jnp.float32)
-                for h in range(up.shape[0])
-            ],
-            axis=0,
+    sides, heads_here = 2, up.shape[0]
+    span = GROUP * BLOCK
+    weights = full.reshape(sides, heads_here, -1, width)
+
+    def weigh(b, side, g):
+        picked = jnp.concatenate([keys[places[b, g * GROUP + i]] for i in range(GROUP)], axis=0)
+        scores = lax.dot_general(
+            picked, queries[b], (((1,), (1,)), ((), ())), preferred_element_type=jnp.float32
         )
-        staged[b] = jnp.transpose(turned).astype(jnp.bfloat16).reshape(peers, group, width)
-        each(1, peers, lambda i: heads_copy(peer(i), b, tp).start())
+        diagonal = jnp.exp2(scores[:BLOCK] + bias[jnp.minimum(g, 1)]).astype(jnp.bfloat16)
+        others = jnp.exp2(scores[BLOCK:]).astype(jnp.bfloat16)
+        for h in range(heads_here):
+            cols = slice(h * BLOCK, (h + 1) * BLOCK)
+            weights[side, h, :BLOCK, :] = diagonal[:, cols]
+            weights[side, h, BLOCK:span, :] = others[:, cols]
+
+    def add_up(b, side, g):
+        held = jnp.concatenate([values[places[b, g * GROUP + i]] for i in range(GROUP)], axis=1)
+        right = jnp.concatenate([weights[side, h, :span, :] for h in range(heads_here)], axis=1)
+        return jnp.dot(held, right, preferred_element_type=jnp.float32)
+
+    def hand_over(b, ended):
+        shares = []
+        for total in ended:
+            shares.append((total[:BLOCK] / total[BLOCK : BLOCK + 1]).astype(jnp.bfloat16))
+        turned, flipped = [], []
+        for side in range(sides):
+            for h in range(heads_here):
+                share = shares[side][:, h * BLOCK : (h + 1) * BLOCK]
+                turned.append(jnp.dot(up[h], share, preferred_element_type=jnp.float32))
+        for side in range(sides):
+            both = jnp.concatenate(turned[side * heads_here : (side + 1) * heads_here], axis=0)
+            flipped.append(jnp.transpose(both).astype(jnp.bfloat16).reshape(peers, group, width))
+        for side in range(sides):
+            staged[b + side] = flipped[side]
+
+    def attend(i):
+        first = sides * i
+        for side in range(sides):
+            weigh(first + side, side, 0)
+            totals[side] = jnp.zeros(totals.shape[1:], jnp.float32)
+
+        def both(g):
+            for side in range(sides):
+                totals[side] = totals[side] + add_up(first + side, side, g - 1)
+            for side in range(sides):
+                weigh(first + side, side, g)
+
+        each(1, picks // GROUP, both)
+        ended = [totals[side] + add_up(first + side, side, picks // GROUP - 1) for side in range(sides)]
+        hand_over(first, ended)
+        for side in range(sides):
+            each(1, peers, lambda j: heads_copy(peer(j), first + side, tp).start())
 
     def out_copy(to, half, slot):
         lower = pl.ds(half * HALF, HALF)
@@ -371,15 +400,15 @@
     def turn(i):
         attend(i)
 
+        @pl.when(i == 1)
+        def _():
+            out_spread.relay_first()
+
         @pl.when(i == 2)
         def _():
-            out_spread.relay_first()
-
-        @pl.when(i == 4)
-        def _():
             out_spread.relay_rest()
 
-    each(0, blocks, turn)
+    each(0, blocks // sides, turn)
     out_spread.finish()
     conclude(0)
     conclude(1)
@@ -432,6 +461,8 @@
             pltpu.VMEM((blocks, heads * BLOCK, width), bf16),
             pltpu.VMEM((slots + 1, BLOCK, width), bf16),
             pltpu.VMEM((slots + 1, BLOCK + ONES, BLOCK), bf16),
+            pltpu.VMEM((2, BLOCK + ONES, heads * BLOCK), jnp.float32),
+            pltpu.VMEM((2, BLOCK, heads * BLOCK), jnp.float32),
             pltpu.SMEM((blocks, picks), jnp.int32),
             pltpu.VMEM((blocks, peers, group, width), bf16),
             pltpu.VMEM((peers, blocks, group, width), bf16),

time: 78.3 us -> 71.9 us (0.918)
  Pallas kernels: 76.5 us -> 70.1 us
    pallas_call x1, Pallas kernels: 76.5 us -> 70.1 us  [shards(): pl.pallas_call(kernel, out_shape=jax.ShapeDtypeStruct((blocks, peers, gro...]
where the time goes in v5:
time: 71.9 us; the launch traced here: 71.8 us
  Pallas kernels  70.1 us (97%)
  local copies, waits for them, and re-layouts  1.67 us (2%)
    pallas_call x1, Pallas kernels, shards(): pl.pallas_call(kernel, out_shape=jax.ShapeDtypeStruct((blocks, peers, gro...  70.1 us
    unnamed x1, local copies, waits for them, and re-layouts  1.67 us

profile of v5, /device:TPU:1, one launch (start us, length us, event | category | flops | bytes accessed | tf_op | source)
XLA Modules:
  0.0 71.8 jit_solution(7707675114114011565)
XLA Ops:
  0.0 70.1 %shard_map.91 = bf16[8,8,16,128]{3,2,1,0:T(8,128)(2,1)} custom-call(s32[8,32]{1,0:T(8,128)} %chosen.1, bf16[8,8,16,128]{3,2,1,0:T(8,128)(2,1)} %bitcast.7, bf16[1024,128]{1,0:T(8,128)(2,1)} %latent_weight.1, bf16[1024,256]{1,0:T(8,128)(2,1)} %query_weight.1, bf16[128,1024]{1,0:T(8,128)(2,1)} %out_weight.1, f32[1,128]{1,0:T(1,128)} %bitcast.10, ...), custom_call_target="tpu_custom_call" | custom-call | tf_op jit(solution)/shard_map/pallas_call | solution.py:444
  70.1 1.7 %copy.11 = bf16[1024,128]{1,0:T(8,128)(2,1)} copy(bf16[1024,128]{1,0:T(8,128)(2,1)} %bitcast.6) | data formatting | bytes 524288

commit v6 on v5

--- a/solution.py
+++ b/solution.py
@@ -37,62 +37,45 @@
         self.tp = lax.axis_index("tp")
         self.right, self.left, self.far, self.other = neighbours(self.tp)
 
-    def copy(self, slot, part, dest, kind):
-        first, size = self.ranges[part]
-        piece = self.full.at[slot, pl.ds(first, size)]
-        return pltpu.make_async_remote_copy(
-            src_ref=piece,
-            dst_ref=piece,
-            send_sem=self.send_sem.at[kind],
-            recv_sem=self.recv_sem.at[slot, part],
-            device_id={"tp": dest},
-            device_id_type=MESH,
-        )
-
     def sends(self):
         me, right, left, far, other = self.tp, self.right, self.left, self.far, self.other
         return (
-            (me, 0, right), (me, 1, left), (me, 1, right), (me, 0, left), (me, 0, other), (me, 1, other),
-            (left, 0, right), (right, 1, left), (left, 0, other), (right, 1, other), (left, 1, other),
-            (right, 0, other), (far, 0, other), (far, 1, other),
+            (me, 0, right, 0), (me, 1, left, 0), (me, 1, right, 1), (me, 0, left, 1), (me, 0, other, 2), (me, 1, other, 2),
+            (left, 0, right, 1), (right, 1, left, 1), (left, 0, other, 2), (right, 1, other, 2), (left, 1, other, 2),
+            (right, 0, other, 2), (far, 0, other, 2), (far, 1, other, 2),
         )
 
     def start(self, *kinds):
         every = self.sends()
         for kind in kinds:
-            self.copy(*every[kind], kind).start()
-
-    def arrived(self, slot, part):
-        self.copy(slot, part, self.other, 0).wait_recv()
+            slot, part, dest, arrival = every[kind]
+            first, size = self.ranges[part]
+            piece = self.full.at[slot, pl.ds(first, size)]
+            remote(piece, piece, self.send_sem, self.recv_sem.at[arrival], "tp", dest).start()
+
+    def slices(self, count, sem):
+        wait_bytes(self.full.at[pl.ds(0, count), pl.ds(self.ranges[0][0], sum(size for _, size in self.ranges))], sem)
 
     def own(self):
         self.start(0, 1, 2, 3, 4, 5)
 
     def relay_first(self):
-        self.arrived(self.left, 0)
-        self.start(6, 8)
-        self.arrived(self.right, 1)
-        self.start(7, 9)
+        self.slices(1, self.recv_sem.at[0])
+        self.start(6, 7, 8, 9)
 
     def relay_rest(self):
-        self.arrived(self.left, 1)
-        self.start(10)
-        self.arrived(self.right, 0)
-        self.start(11)
-        self.arrived(self.far, 0)
-        self.start(12)
-        self.arrived(self.far, 1)
-        self.start(13)
+        self.slices(2, self.recv_sem.at[1])
+        self.start(10, 11, 12, 13)
 
     def finish(self):
-        side = 1 - 2 * lax.rem(self.tp, 2)
-        for slot in (self.other, self.left + side, self.right + side, self.far + side):
-            for part in (0, 1):
-                self.arrived(slot, part)
+        self.slices(4, self.recv_sem.at[2])
 
     def drain(self):
-        for kind, (slot, part, dest) in enumerate(self.sends()):
-            self.copy(slot, part, dest, kind).wait_send()
+        self.slices(7, self.send_sem)
+
+
+def wait_bytes(region, sem):
+    pltpu.make_async_copy(region, region, sem).wait()
 
 
 def each(low, high, act):
@@ -120,8 +103,9 @@
 
 
 def kernel(
-    chosen, tokens, latent_weight, query_weight, out_weight, query_gain, key_gain, up, out_gain,
+    chosen_in, tokens, latent_weight, query_weight, out_weight, query_gain_in, key_gain_in, up_in, out_gain_in,
     out,
+    chosen, query_gain, key_gain, up, out_gain,
     full, pool, wide_weight, weight, projection, rows, asked, asks, served, listed, table,
     queries, keys, values, totals, bias, places, staged, heads,
     local_sem, rows_send, rows_recv, ask_send, ask_recv, serve_send, serve_recv,
@@ -138,9 +122,14 @@
     own_latent = pltpu.make_async_copy(latent_weight, weight, local_sem.at[1])
     own_query = pltpu.make_async_copy(query_weight, projection, local_sem.at[2])
     own_out = pltpu.make_async_copy(out_weight, wide_weight.at[tp], local_sem.at[3])
-    for copy in (own_tokens, own_latent, own_query, own_out):
-        copy.start()
-
+    small = [
+        pltpu.make_async_copy(source, target, local_sem.at[5 + i])
+        for i, (source, target) in enumerate(
+            (
+                (chosen_in, chosen), (query_gain_in, query_gain), (key_gain_in, key_gain), (up_in, up), (out_gain_in, out_gain)
+            )
+        )
+    ]
     barrier = pltpu.get_barrier_semaphore()
 
     def greet(axis, index, size):
@@ -152,18 +141,22 @@
     greet("kv", kv, owners)
     greet("tp", tp, peers)
 
+    for copy in (own_tokens, *small, own_latent, own_query, own_out):
+        copy.start()
     own_tokens.wait()
     pl.semaphore_wait(barrier, owners + peers - 2)
 
+    share = owners // PIECES
+
     def rows_copy(to, slot):
-        return remote(full.at[tp, :, to], rows.at[slot], rows_send.at[to], rows_recv.at[slot], "tp", to)
+        return remote(full.at[tp, :, to], rows.at[slot], rows_send, rows_recv, "tp", to)
 
     def ask_copy(to, slot):
-        return remote(asks.at[to], asked.at[slot], ask_send.at[to], ask_recv.at[slot], "kv", to)
+        return remote(asks.at[to], asked.at[slot], ask_send, ask_recv, "kv", to)
 
     def serve_copy(to, slot):
         target = pool.at[tp, pl.ds(blocks + slot * PER_OWNER, PER_OWNER)]
-        return remote(served.at[to], target, serve_send.at[to], serve_recv.at[slot], "kv", to)
+        return remote(served.at[to], target, serve_send, serve_recv.at[lax.div(slot, share)], "kv", to)
 
     def peer(i):
         return lax.rem(tp + i, peers)
@@ -178,6 +171,8 @@
     lane = lax.broadcasted_iota(jnp.int32, tile, 1)
     sub = lax.broadcasted_iota(jnp.int32, tile, 0)
     ids = lane * blocks + sub
+
+    small[0].wait()
 
     def mark(b, needed):
         for c in range(picks):
@@ -197,9 +192,15 @@
     to_scalars.start()
     both = both.astype(jnp.float32)
 
-    for o in range(owners - 1):
-        asks[o] = jnp.broadcast_to(jnp.sum(jnp.where(lane == o, both, 0.0), axis=1, keepdims=True), tile)
-    each(0, kv, lambda o: ask_copy(o, kv).start())
+    for o in range(owners):
+        spread_out = jnp.sum(jnp.where(lane == o, both, 0.0), axis=1, keepdims=True)
+        asks[o] = jnp.broadcast_to(spread_out, tile)[:PER_OWNER]
+    others = owners - 1
+
+    def owner_at(i):
+        return lax.rem(kv + i, owners)
+
+    each(1, owners, lambda i: ask_copy(owner_at(i), kv).start())
 
     ones = jnp.ones((ONES, BLOCK), jnp.bfloat16)
 
@@ -213,65 +214,6 @@
     bias[1] = jnp.zeros(bias.shape[1:], jnp.float32)
     keys[slots] = jnp.zeros((BLOCK, width), jnp.bfloat16)
     values[slots] = jnp.zeros((BLOCK + ONES, BLOCK), jnp.bfloat16)
-    rows[tp] = full[tp, :, tp]
-    own_latent.wait()
-    each(1, peers, lambda i: rows_copy(peer(i), peer(i)).wait_recv())
-    @jax.jit
-    def compress():
-        features = jnp.concatenate([rows[p].reshape(lines, width) for p in range(peers)], axis=1)
-        latent = jnp.dot(features, weight[...], preferred_element_type=jnp.float32)
-        return latent.astype(jnp.bfloat16).reshape(blocks, group, 128)
-
-    latent = compress()
-    pool[tp, 0:blocks] = latent
-    latent = latent.astype(jnp.float32)
-
-    def serve(i):
-        r = owners - 1 - i
-        ask_copy(r, r).wait_recv()
-        for k in range(PER_OWNER):
-            want = asked[r, k : k + 1, :]
-            picked = jnp.zeros((group, 128), jnp.float32)
-            for j in range(blocks):
-                picked = jnp.where(want == float(j), latent[j], picked)
-            served[r, k] = picked.astype(jnp.bfloat16)
-        serve_copy(r, kv).start()
-
-    each(0, owners - 1 - kv, serve)
-    here = Spread(pool, 0, blocks, spread_send.at[1], spread_recv.at[1])
-    here.own()
-
-    share = owners // PIECES
-    spreads = [
-        Spread(pool, blocks + i * share * PER_OWNER, share * PER_OWNER, spread_send.at[2 + i], spread_recv.at[2 + i])
-        for i in range(PIECES)
-    ]
-
-    def gathered(i):
-        low = i * share
-        each(low, jnp.clip(kv, low, low + share), lambda o: serve_copy(o, o).wait_recv())
-        spreads[i].own()
-
-    scale = width ** (-0.5) * LOG2E
-    query_row = query_gain[...] * scale
-
-    def project(b):
-        features = jnp.concatenate([full[p, b].reshape(BLOCK, width) for p in range(peers)], axis=1)
-        projected = jnp.dot(features, projection[...], preferred_element_type=jnp.float32)
-        projected = projected.astype(jnp.bfloat16).astype(jnp.float32)
-        for h in range(up.shape[0]):
-            queries[b, h * BLOCK : (h + 1) * BLOCK, :] = unit(projected[:, h * 128 : (h + 1) * 128], query_row)
-
-    def prepare(low, high):
-        def several(j):
-            for i in range(4):
-                slot = low + 4 * j + i
-                block = pool[:, slot].reshape(BLOCK, width).astype(jnp.float32)
-                keys[slot] = unit(block, key_gain[...])
-                values[slot, :BLOCK, :] = jnp.transpose(block).astype(jnp.bfloat16)
-
-        each(0, (high - low) // 4, several)
-
     def place(b):
         for c in range(picks):
             block = chosen[b, c]
@@ -282,10 +224,75 @@
             places[b, c] = jnp.where(block < 0, slots, jnp.where(owner == kv, inside, away))
 
     to_scalars.wait()
-    each(1, peers, lambda i: rows_copy(peer(i), tp).wait_send())
     each(0, blocks, place)
-    own_query.wait()
-    own_out.wait()
+    for copy in small[1:]:
+        copy.wait()
+    rows[tp] = full[tp, :, tp]
+    own_latent.wait()
+    wait_bytes(rows.at[pl.ds(0, peers - 1)], rows_recv)
+
+    @jax.jit
+    def compress():
+        features = jnp.concatenate([rows[p].reshape(lines, width) for p in range(peers)], axis=1)
+        latent = jnp.dot(features, weight[...], preferred_element_type=jnp.float32)
+        return latent.astype(jnp.bfloat16).reshape(blocks, group, 128)
+
+    latent = compress()
+    pool[tp, 0:blocks] = latent
+    latent = latent.astype(jnp.float32)
+
+    def serve(i):
+        r = owner_at(i)
+        for k in range(PER_OWNER):
+            want = asked[r, k : k + 1, :]
+            picked = jnp.zeros((group, 128), jnp.float32)
+            for j in range(blocks):
+                picked = jnp.where(want == float(j), latent[j], picked)
+            served[r, k] = picked.astype(jnp.bfloat16)
+        serve_copy(r, kv).start()
+
+    wait_bytes(asked.at[pl.ds(0, others)], ask_recv)
+    each(owners // 2, owners, serve)
+    each(1, owners // 2, serve)
+    pltpu.make_async_copy(
+        pool.at[tp, pl.ds(0, PER_OWNER)],
+        pool.at[tp, pl.ds(blocks + kv * PER_OWNER, PER_OWNER)],
+        serve_recv.at[lax.div(kv, share)],
+    ).start()
+    here = Spread(pool, 0, blocks, spread_send.at[1], spread_recv.at[1])
+    here.own()
+
+    spreads = [
+        Spread(pool, blocks + i * share * PER_OWNER, share * PER_OWNER, spread_send.at[2 + i], spread_recv.at[2 + i])
+        for i in range(PIECES)
+    ]
+
+    def gathered(i):
+        per_piece = share * PER_OWNER
+        wait_bytes(pool.at[tp, pl.ds(blocks + i * per_piece, per_piece)], serve_recv.at[i])
+        spreads[i].own()
+
+    scale = width ** (-0.5) * LOG2E
+    query_row = query_gain[...] * scale
+
+    def project(b):
+        features = jnp.concatenate([full[p, b].reshape(BLOCK, width) for p in range(peers)], axis=1)
+        projected = jnp.dot(features, projection[...], preferred_element_type=jnp.float32)
+        projected = projected.astype(jnp.bfloat16).astype(jnp.float32)
+        for h in range(up.shape[0]):
+            queries[b, h * BLOCK : (h + 1) * BLOCK, :] = unit(projected[:, h * 128 : (h + 1) * 128], query_row)
+
+    def prepare(low, high):
+        def several(j):
+            for i in range(4):
+                slot = low + 4 * j + i
+                block = pool[:, slot].reshape(BLOCK, width).astype(jnp.float32)
+                keys[slot] = unit(block, key_gain[...])
+                values[slot, :BLOCK, :] = jnp.transpose(block).astype(jnp.bfloat16)
+
+        each(0, (high - low) // 4, several)
+
+    wait_bytes(rows.at[pl.ds(0, peers - 1)], rows_send)
     token_spread.relay_first()
     here.relay_first()
     for i in range(PIECES):
@@ -293,14 +300,13 @@
     here.relay_rest()
     token_spread.relay_rest()
     token_spread.finish()
-    token_spread.drain()
     here.finish()
-    step = blocks // PIECES
-    for i in range(PIECES):
-        spreads[i].relay_first()
-        each(i * step, (i + 1) * step, project)
-        if i == 0:
-            prepare(0, blocks)
+    for spread in spreads:
+        spread.relay_first()
+    own_query.wait()
+    own_out.wait()
+    each(0, blocks, project)
+    prepare(0, blocks)
     out_spread = Spread(wide_weight, 0, 128, spread_send.at[2 + PIECES], spread_recv.at[2 + PIECES])
     for i in range(PIECES):
         spreads[i].relay_rest()
@@ -308,9 +314,10 @@
             out_spread.own()
         spreads[i].finish()
         prepare(blocks + i * share * PER_OWNER, blocks + (i + 1) * share * PER_OWNER)
+    token_spread.drain()
 
     def heads_copy(to, b, slot):
-        return remote(staged.at[b, to], heads.at[slot, b], heads_send.at[to, b], heads_recv.at[slot, b], "tp", to)
+        return remote(staged.at[b, to], heads.at[slot, b], heads_send, heads_recv.at[lax.div(b, HALF)], "tp", to)
 
     sides, heads_here = 2, up.shape[0]
     span = GROUP * BLOCK
@@ -369,7 +376,7 @@
     def out_copy(to, half, slot):
         lower = pl.ds(half * HALF, HALF)
         return remote(
-            rows.at[to, lower], out.at[lower, slot], out_send.at[to, half], out_recv.at[slot, half], "tp", to
+            rows.at[to, lower], out.at[lower, slot], out_send, out_recv, "tp", to
         )
 
     @functools.partial(jax.jit, static_argnums=0)
@@ -386,11 +393,7 @@
     def conclude(half):
         lower = pl.ds(half * HALF, HALF)
 
-        def landed(i):
-            for b in range(HALF):
-                heads_copy(peer(i), half * HALF + b, peer(i)).wait_recv()
-
-        each(1, peers, landed)
+        wait_bytes(heads.at[pl.ds(0, peers - 1), lower], heads_recv.at[half])
         for b in range(HALF):
             heads[tp, half * HALF + b] = staged[half * HALF + b, tp]
         mix(half)
@@ -400,7 +403,7 @@
     def turn(i):
         attend(i)
 
-        @pl.when(i == 1)
+        @pl.when(i == 0)
         def _():
             out_spread.relay_first()
 
@@ -413,19 +416,13 @@
     conclude(0)
     conclude(1)
 
-    each(0, kv, lambda o: ask_copy(o, kv).wait_send())
-    each(kv + 1, owners, lambda r: serve_copy(r, kv).wait_send())
+    wait_bytes(asks.at[pl.ds(0, others)], ask_send)
+    wait_bytes(served.at[pl.ds(0, others)], serve_send)
     for spread in (here, out_spread, *spreads):
         spread.drain()
-
-    def settle(i):
-        for b in range(blocks):
-            heads_copy(peer(i), b, tp).wait_send()
-        for half in range(2):
-            out_copy(peer(i), half, tp).wait_send()
-            out_copy(peer(i), half, peer(i)).wait_recv()
-
-    each(1, peers, settle)
+    wait_bytes(staged.at[:, pl.ds(0, peers - 1)], heads_send)
+    wait_bytes(rows.at[pl.ds(0, peers - 1)], out_send)
+    wait_bytes(out.at[:, pl.ds(0, peers - 1)], out_recv)
 
 
 def shards(
@@ -444,17 +441,22 @@
     mixed = pl.pallas_call(
         kernel,
         out_shape=jax.ShapeDtypeStruct((blocks, peers, group, width), bf16),
-        in_specs=[pl.BlockSpec(memory_space=pltpu.SMEM)] + [anywhere] * 4 + [vmem] * 4,
+        in_specs=[anywhere] * 9,
         out_specs=vmem,
         scratch_shapes=[
+            pltpu.SMEM((blocks, picks), jnp.int32),
+            pltpu.VMEM((1, width), jnp.float32),
+            pltpu.VMEM((1, width), jnp.float32),
+            pltpu.VMEM((heads, value_up.shape[2], width), bf16),
+            pltpu.VMEM((1, out_gain.shape[0]), jnp.float32),
             pltpu.VMEM((peers, blocks, peers, group, width), bf16),
             pltpu.VMEM((peers, slots, group, width), bf16),
             pltpu.VMEM((peers, *out_weight.shape), bf16),
             pltpu.VMEM(latent_weight.shape, bf16),
             pltpu.VMEM(query_weight.shape, bf16),
             pltpu.VMEM((peers, blocks, group, width), bf16),
-            pltpu.VMEM((owners, blocks, 128), jnp.float32),
-            pltpu.VMEM((owners, blocks, 128), jnp.float32),
+            pltpu.VMEM((owners, PER_OWNER, 128), jnp.float32),
+            pltpu.VMEM((owners, PER_OWNER, 128), jnp.float32),
             pltpu.VMEM((owners, PER_OWNER, group, width), bf16),
             pltpu.VMEM((blocks, 128), jnp.int32),
             pltpu.SMEM((blocks, 128), jnp.int32),
@@ -466,13 +468,13 @@
             pltpu.SMEM((blocks, picks), jnp.int32),
             pltpu.VMEM((blocks, peers, group, width), bf16),
             pltpu.VMEM((peers, blocks, group, width), bf16),
-            dma((5,)),
-            dma((peers,)), dma((peers,)),
-            dma((owners,)), dma((owners,)),
-            dma((owners,)), dma((owners,)),
-            dma((peers, blocks)), dma((peers, blocks)),
-            dma((peers, 2)), dma((peers, 2)),
-            dma((3 + PIECES, 14)), dma((3 + PIECES, peers, 2)),
+            dma((10,)),
+            dma, dma,
+            dma, dma,
+            dma, dma((PIECES,)),
+            dma, dma((2,)),
+            dma, dma,
+            dma((3 + PIECES,)), dma((3 + PIECES, 3)),
         ],
         compiler_params=pltpu.CompilerParams(collective_id=0, has_side_effects=True),
     )(

time: 71.9 us -> 68.3 us (0.950)
  Pallas kernels: 70.1 us -> 66.5 us
    pallas_call x1, Pallas kernels: 70.1 us -> 66.5 us  [shards(): pl.pallas_call(kernel, out_shape=jax.ShapeDtypeStruct((blocks, peers, gro...]
where the time goes in v6:
time: 68.3 us; the launch traced here: 68.2 us
  Pallas kernels  66.5 us (97%)
  local copies, waits for them, and re-layouts  1.67 us (2%)
    pallas_call x1, Pallas kernels, shards(): pl.pallas_call(kernel, out_shape=jax.ShapeDtypeStruct((blocks, peers, gro...  66.5 us
    unnamed x1, local copies, waits for them, and re-layouts  1.67 us

profile of v6, /device:TPU:1, one launch (start us, length us, event | category | flops | bytes accessed | tf_op | source)
XLA Modules:
  0.0 68.2 jit_solution(15497624132712734171)
XLA Ops:
  0.0 66.5 %shard_map.91 = bf16[8,8,16,128]{3,2,1,0:T(8,128)(2,1)} custom-call(s32[8,32]{1,0:T(8,128)} %chosen_in.1, bf16[8,8,16,128]{3,2,1,0:T(8,128)(2,1)} %bitcast.7, bf16[1024,128]{1,0:T(8,128)(2,1)} %latent_weight.1, bf16[1024,256]{1,0:T(8,128)(2,1)} %query_weight.1, bf16[128,1024]{1,0:T(8,128)(2,1)} %out_weight.1, f32[1,128]{1,0:T(1,128)} %bitcast.10, ...), custom_call_target="tpu_custom_call" | custom-call | tf_op jit(solution)/shard_map/pallas_call | solution.py:441
  66.5 1.7 %copy.11 = bf16[1024,128]{1,0:T(8,128)(2,1)} copy(bf16[1024,128]{1,0:T(8,128)(2,1)} %bitcast.6) | data formatting | bytes 524288

commit v7 on v6

--- a/solution.py
+++ b/solution.py
@@ -154,9 +154,11 @@
     def ask_copy(to, slot):
         return remote(asks.at[to], asked.at[slot], ask_send, ask_recv, "kv", to)
 
+    def serve_target(slot):
+        return pool.at[tp, pl.ds(blocks + slot * PER_OWNER, PER_OWNER)]
+
     def serve_copy(to, slot):
-        target = pool.at[tp, pl.ds(blocks + slot * PER_OWNER, PER_OWNER)]
-        return remote(served.at[to], target, serve_send, serve_recv.at[lax.div(slot, share)], "kv", to)
+        return remote(served.at[to], serve_target(slot), serve_send, serve_recv.at[lax.div(slot, share)], "kv", to)
 
     def peer(i):
         return lax.rem(tp + i, peers)
@@ -197,10 +199,12 @@
         asks[o] = jnp.broadcast_to(spread_out, tile)[:PER_OWNER]
     others = owners - 1
 
-    def owner_at(i):
-        return lax.rem(kv + i, owners)
-
-    each(1, owners, lambda i: ask_copy(owner_at(i), kv).start())
+    def stay(source, target, sem):
+        pltpu.make_async_copy(source, target, sem).start()
+
+    each(0, kv, lambda o: ask_copy(o, kv).start())
+    each(0, kv, lambda o: stay(asks.at[kv], asked.at[o], ask_recv))
+    each(kv + 1, owners, lambda o: stay(asks.at[kv], asks.at[o], ask_send))
 
     ones = jnp.ones((ONES, BLOCK), jnp.bfloat16)
 
@@ -242,7 +246,7 @@
     latent = latent.astype(jnp.float32)
 
     def serve(i):
-        r = owner_at(i)
+        r = others - i
         for k in range(PER_OWNER):
             want = asked[r, k : k + 1, :]
             picked = jnp.zeros((group, 128), jnp.float32)
@@ -252,13 +256,10 @@
         serve_copy(r, kv).start()
 
     wait_bytes(asked.at[pl.ds(0, others)], ask_recv)
-    each(owners // 2, owners, serve)
-    each(1, owners // 2, serve)
-    pltpu.make_async_copy(
-        pool.at[tp, pl.ds(0, PER_OWNER)],
-        pool.at[tp, pl.ds(blocks + kv * PER_OWNER, PER_OWNER)],
-        serve_recv.at[lax.div(kv, share)],
-    ).start()
+    each(0, others - kv, serve)
+    low = pool.at[tp, pl.ds(0, PER_OWNER)]
+    each(0, kv, lambda o: stay(low, served.at[o], serve_send))
+    each(kv, owners, lambda o: stay(low, serve_target(o), serve_recv.at[lax.div(o, share)]))
     here = Spread(pool, 0, blocks, spread_send.at[1], spread_recv.at[1])
     here.own()
 
@@ -294,24 +295,24 @@
 
     wait_bytes(rows.at[pl.ds(0, peers - 1)], rows_send)
     token_spread.relay_first()
-    here.relay_first()
+    token_spread.relay_rest()
     for i in range(PIECES):
         gathered(i)
+    token_spread.finish()
+    own_query.wait()
+    own_out.wait()
+    here.relay_first()
+    each(0, blocks, project)
     here.relay_rest()
-    token_spread.relay_rest()
-    token_spread.finish()
-    here.finish()
     for spread in spreads:
         spread.relay_first()
-    own_query.wait()
-    own_out.wait()
-    each(0, blocks, project)
+    here.finish()
     prepare(0, blocks)
     out_spread = Spread(wide_weight, 0, 128, spread_send.at[2 + PIECES], spread_recv.at[2 + PIECES])
+    for spread in spreads:
+        spread.relay_rest()
+    out_spread.own()
     for i in range(PIECES):
-        spreads[i].relay_rest()
-        if i == PIECES - 1:
-            out_spread.own()
         spreads[i].finish()
         prepare(blocks + i * share * PER_OWNER, blocks + (i + 1) * share * PER_OWNER)
     token_spread.drain()
@@ -403,11 +404,11 @@
     def turn(i):
         attend(i)
 
-        @pl.when(i == 0)
+        @pl.when(i == 1)
         def _():
             out_spread.relay_first()
 
-        @pl.when(i == 2)
+        @pl.when(i == 3)
         def _():
             out_spread.relay_rest()
 

time: 68.3 us -> 64.7 us (0.947)
  Pallas kernels: 66.5 us -> 62.9 us
    pallas_call x1, Pallas kernels: 66.5 us -> 62.9 us  [shards(): pl.pallas_call(kernel, out_shape=jax.ShapeDtypeStruct((blocks, peers, gro...]
where the time goes in v7:
time: 64.7 us; the launch traced here: 64.5 us
  Pallas kernels  62.9 us (97%)
  local copies, waits for them, and re-layouts  1.67 us (3%)
    pallas_call x1, Pallas kernels, shards(): pl.pallas_call(kernel, out_shape=jax.ShapeDtypeStruct((blocks, peers, gro...  62.9 us
    unnamed x1, local copies, waits for them, and re-layouts  1.67 us

profile of v7, /device:TPU:1, one launch (start us, length us, event | category | flops | bytes accessed | tf_op | source)
XLA Modules:
  0.0 64.5 jit_solution(11700511998977204339)
XLA Ops:
  0.0 62.9 %shard_map.91 = bf16[8,8,16,128]{3,2,1,0:T(8,128)(2,1)} custom-call(s32[8,32]{1,0:T(8,128)} %chosen_in.1, bf16[8,8,16,128]{3,2,1,0:T(8,128)(2,1)} %bitcast.7, bf16[1024,128]{1,0:T(8,128)(2,1)} %latent_weight.1, bf16[1024,256]{1,0:T(8,128)(2,1)} %query_weight.1, bf16[128,1024]{1,0:T(8,128)(2,1)} %out_weight.1, f32[1,128]{1,0:T(1,128)} %bitcast.10, ...), custom_call_target="tpu_custom_call" | custom-call | tf_op jit(solution)/shard_map/pallas_call | solution.py:442
  62.9 1.7 %copy.11 = bf16[1024,128]{1,0:T(8,128)(2,1)} copy(bf16[1024,128]{1,0:T(8,128)(2,1)} %bitcast.6) | data formatting | bytes 524288

commit v8 on v7

--- a/solution.py
+++ b/solution.py
@@ -295,26 +295,31 @@
 
     wait_bytes(rows.at[pl.ds(0, peers - 1)], rows_send)
     token_spread.relay_first()
+    here.relay_first()
     token_spread.relay_rest()
     for i in range(PIECES):
         gathered(i)
     token_spread.finish()
     own_query.wait()
     own_out.wait()
-    here.relay_first()
     each(0, blocks, project)
-    here.relay_rest()
     for spread in spreads:
         spread.relay_first()
+    out_spread = Spread(wide_weight, 0, 128, spread_send.at[2 + PIECES], spread_recv.at[2 + PIECES])
+    out_spread.own()
+    here.relay_rest()
     here.finish()
     prepare(0, blocks)
-    out_spread = Spread(wide_weight, 0, 128, spread_send.at[2 + PIECES], spread_recv.at[2 + PIECES])
-    for spread in spreads:
-        spread.relay_rest()
-    out_spread.own()
-    for i in range(PIECES):
+
+    def complete(i):
         spreads[i].finish()
         prepare(blocks + i * share * PER_OWNER, blocks + (i + 1) * share * PER_OWNER)
+
+    spreads[0].relay_rest()
+    for i in range(1, PIECES):
+        spreads[i].relay_rest()
+        complete(i - 1)
+    complete(PIECES - 1)
     token_spread.drain()
 
     def heads_copy(to, b, slot):
@@ -356,10 +361,13 @@
         for side in range(sides):
             staged[b + side] = flipped[side]
 
-    def attend(i):
+    def start(i):
+        for side in range(sides):
+            weigh(sides * i + side, side, 0)
+
+    def attend(i, following):
         first = sides * i
         for side in range(sides):
-            weigh(first + side, side, 0)
             totals[side] = jnp.zeros(totals.shape[1:], jnp.float32)
 
         def both(g):
@@ -370,6 +378,8 @@
 
         each(1, picks // GROUP, both)
         ended = [totals[side] + add_up(first + side, side, picks // GROUP - 1) for side in range(sides)]
+        if following:
+            start(i + 1)
         hand_over(first, ended)
         for side in range(sides):
             each(1, peers, lambda j: heads_copy(peer(j), first + side, tp).start())
@@ -402,19 +412,22 @@
         out[lower, tp] = rows[tp, lower]
 
     def turn(i):
-        attend(i)
-
-        @pl.when(i == 1)
+        attend(i, True)
+
+        @pl.when(i == 0)
         def _():
             out_spread.relay_first()
 
-        @pl.when(i == 3)
+        @pl.when(i == 2)
         def _():
             out_spread.relay_rest()
-
-    each(0, blocks // sides, turn)
-    out_spread.finish()
-    conclude(0)
+            out_spread.finish()
+            conclude(0)
+
+    last = blocks // sides - 1
+    each(0, 1, start)
+    each(0, last, turn)
+    each(last, last + 1, lambda i: attend(i, False))
     conclude(1)
 
     wait_bytes(asks.at[pl.ds(0, others)], ask_send)

time: 64.7 us -> 64.5 us (level)
  no operation moved by 1% of the time
where the time goes in v8:
time: 64.5 us; the launch traced here: 64.4 us
  Pallas kernels  62.7 us (97%)
  local copies, waits for them, and re-layouts  1.67 us (3%)
    pallas_call x1, Pallas kernels, shards(): pl.pallas_call(kernel, out_shape=jax.ShapeDtypeStruct((blocks, peers, gro...  62.7 us
    unnamed x1, local copies, waits for them, and re-layouts  1.67 us

profile of v8, /device:TPU:1, one launch (start us, length us, event | category | flops | bytes accessed | tf_op | source)
XLA Modules:
  0.0 64.4 jit_solution(3807564309735640618)
XLA Ops:
  0.0 62.7 %shard_map.91 = bf16[8,8,16,128]{3,2,1,0:T(8,128)(2,1)} custom-call(s32[8,32]{1,0:T(8,128)} %chosen_in.1, bf16[8,8,16,128]{3,2,1,0:T(8,128)(2,1)} %bitcast.7, bf16[1024,128]{1,0:T(8,128)(2,1)} %latent_weight.1, bf16[1024,256]{1,0:T(8,128)(2,1)} %query_weight.1, bf16[128,1024]{1,0:T(8,128)(2,1)} %out_weight.1, f32[1,128]{1,0:T(1,128)} %bitcast.10, ...), custom_call_target="tpu_custom_call" | custom-call | tf_op jit(solution)/shard_map/pallas_call | solution.py:455
  62.7 1.7 %copy.11 = bf16[1024,128]{1,0:T(8,128)(2,1)} copy(bf16[1024,128]{1,0:T(8,128)(2,1)} %bitcast.6) | data formatting | bytes 524288

commit v9 on v8

--- a/solution.py
+++ b/solution.py
@@ -271,7 +271,7 @@
     def gathered(i):
         per_piece = share * PER_OWNER
         wait_bytes(pool.at[tp, pl.ds(blocks + i * per_piece, per_piece)], serve_recv.at[i])
-        spreads[i].own()
+        spreads[i].start(0, 1)
 
     scale = width ** (-0.5) * LOG2E
     query_row = query_gain[...] * scale
@@ -296,9 +296,11 @@
     wait_bytes(rows.at[pl.ds(0, peers - 1)], rows_send)
     token_spread.relay_first()
     here.relay_first()
-    token_spread.relay_rest()
     for i in range(PIECES):
         gathered(i)
+    for spread in spreads:
+        spread.start(2, 3, 4, 5)
+    token_spread.relay_rest()
     token_spread.finish()
     own_query.wait()
     own_out.wait()
@@ -421,13 +423,13 @@
         @pl.when(i == 2)
         def _():
             out_spread.relay_rest()
-            out_spread.finish()
-            conclude(0)
 
     last = blocks // sides - 1
     each(0, 1, start)
     each(0, last, turn)
     each(last, last + 1, lambda i: attend(i, False))
+    out_spread.finish()
+    conclude(0)
     conclude(1)
 
     wait_bytes(asks.at[pl.ds(0, others)], ask_send)
@@ -454,7 +456,7 @@
     bf16 = jnp.bfloat16
     mixed = pl.pallas_call(
         kernel,
-        out_shape=jax.ShapeDtypeStruct((blocks, peers, group, width), bf16),
+        out_shape=pltpu.VMEM((blocks, peers, group, width), bf16),
         in_specs=[anywhere] * 9,
         out_specs=vmem,
         scratch_shapes=[

time: 64.5 us -> 61 us (0.946)
  Pallas kernels: 62.7 us -> 60.2 us
  local copies, waits for them, and re-layouts: 1.67 us -> 0.71 us
    pallas_call x1, Pallas kernels: 62.7 us -> 60.2 us  [shards(): pl.pallas_call(kernel, out_shape=pltpu.VMEM((blocks, peers, group, width)...]
    unnamed x1, local copies, waits for them, and re-layouts: 1.67 us -> 0.71 us
where the time goes in v9:
time: 61 us; the launch traced here: 60.9 us
  Pallas kernels  60.2 us (99%)
  local copies, waits for them, and re-layouts  0.71 us (1%)
    pallas_call x1, Pallas kernels, shards(): pl.pallas_call(kernel, out_shape=pltpu.VMEM((blocks, peers, group, width)...  60.2 us

profile of v9, /device:TPU:1, one launch (start us, length us, event | category | flops | bytes accessed | tf_op | source)
XLA Modules:
  0.0 60.9 jit_solution(2150193615033346910)
XLA Ops:
  0.0 60.2 %shard_map.91 = bf16[8,8,16,128]{3,2,1,0:T(8,128)(2,1)S(1)} custom-call(s32[8,32]{1,0:T(8,128)} %chosen_in.1, bf16[8,8,16,128]{3,2,1,0:T(8,128)(2,1)} %bitcast.7, bf16[1024,128]{1,0:T(8,128)(2,1)} %latent_weight.1, bf16[1024,256]{1,0:T(8,128)(2,1)} %query_weight.1, bf16[128,1024]{1,0:T(8,128)(2,1)} %out_weight.1, f32[1,128]{1,0:T(1,128)} %bitcast.10, ...), custom_call_target="tpu_custom_call" | custom-call | tf_op jit(solution)/shard_map/pallas_call | solution.py:457
  60.2 0.7 %copy.11 = bf16[1024,128]{1,0:T(8,128)(2,1)} copy(bf16[1024,128]{1,0:T(8,128)(2,1)S(1)} %bitcast.6) | data formatting | bytes 524288

commit v10 on v9

--- a/solution.py
+++ b/solution.py
@@ -13,7 +13,7 @@
 GROUP = 8
 PIECES = 4
 ONES = 16
-HALF = 4
+HALF = 6
 LOG2E = 1.4426950408889634
 
 
@@ -283,13 +283,20 @@
         for h in range(up.shape[0]):
             queries[b, h * BLOCK : (h + 1) * BLOCK, :] = unit(projected[:, h * 128 : (h + 1) * 128], query_row)
 
+    eye_shape = (BLOCK, BLOCK)
+    same = lax.broadcasted_iota(jnp.int32, eye_shape, 0) == lax.broadcasted_iota(jnp.int32, eye_shape, 1)
+    eye = jnp.where(same, 1.0, 0.0).astype(jnp.bfloat16)
+
     def prepare(low, high):
         def several(j):
+            first = low + 4 * j
+            picked = [pool[:, first + i].reshape(BLOCK, width) for i in range(4)]
+            turned = lax.dot_general(
+                eye, jnp.concatenate(picked, axis=0), (((1,), (1,)), ((), ())), preferred_element_type=jnp.float32
+            ).astype(jnp.bfloat16)
             for i in range(4):
-                slot = low + 4 * j + i
-                block = pool[:, slot].reshape(BLOCK, width).astype(jnp.float32)
-                keys[slot] = unit(block, key_gain[...])
-                values[slot, :BLOCK, :] = jnp.transpose(block).astype(jnp.bfloat16)
+                keys[first + i] = unit(picked[i].astype(jnp.float32), key_gain[...])
+                values[first + i, :BLOCK, :] = turned[:, i * BLOCK : (i + 1) * BLOCK]
 
         each(0, (high - low) // 4, several)
 
@@ -386,29 +393,30 @@
         for side in range(sides):
             each(1, peers, lambda j: heads_copy(peer(j), first + side, tp).start())
 
+    def part(half):
+        return (0, HALF) if half == 0 else (HALF, blocks - HALF)
+
     def out_copy(to, half, slot):
-        lower = pl.ds(half * HALF, HALF)
-        return remote(
-            rows.at[to, lower], out.at[lower, slot], out_send, out_recv, "tp", to
-        )
+        lower = pl.ds(*part(half))
+        return remote(rows.at[to, lower], out.at[lower, slot], out_send, out_recv, "tp", to)
 
     @functools.partial(jax.jit, static_argnums=0)
     def mix(half):
-        lower = pl.ds(half * HALF, HALF)
-        features = jnp.concatenate([heads[p, lower].reshape(HALF * group, width) for p in range(peers)], axis=1)
+        lower, count = pl.ds(*part(half)), part(half)[1]
+        features = jnp.concatenate([heads[p, lower].reshape(count * group, width) for p in range(peers)], axis=1)
         summed = jnp.dot(
             features, wide_weight[...].reshape(peers * 128, peers * 128), preferred_element_type=jnp.float32
         )
         mixed = unit(summed, out_gain[...])
         for t in range(peers):
-            rows[t, lower] = mixed[:, t * 128 : (t + 1) * 128].reshape(HALF, group, 128)
+            rows[t, lower] = mixed[:, t * 128 : (t + 1) * 128].reshape(count, group, 128)
 
     def conclude(half):
-        lower = pl.ds(half * HALF, HALF)
-
+        first, count = part(half)
+        lower = pl.ds(first, count)
         wait_bytes(heads.at[pl.ds(0, peers - 1), lower], heads_recv.at[half])
-        for b in range(HALF):
-            heads[tp, half * HALF + b] = staged[half * HALF + b, tp]
+        for b in range(first, first + count):
+            heads[tp, b] = staged[b, tp]
         mix(half)
         each(1, peers, lambda i: out_copy(peer(i), half, tp).start())
         out[lower, tp] = rows[tp, lower]

time: 61 us -> 60.4 us (level)
    pallas_call x1, Pallas kernels: 60.2 us -> 59.6 us  [shards(): pl.pallas_call(kernel, out_shape=pltpu.VMEM((blocks, peers, group, width)...]
where the time goes in v10:
time: 60.4 us; the launch traced here: 60.3 us
  Pallas kernels  59.6 us (99%)
  local copies, waits for them, and re-layouts  0.71 us (1%)
    pallas_call x1, Pallas kernels, shards(): pl.pallas_call(kernel, out_shape=pltpu.VMEM((blocks, peers, group, width)...  59.6 us

profile of v10, /device:TPU:1, one launch (start us, length us, event | category | flops | bytes accessed | tf_op | source)
XLA Modules:
  0.0 60.3 jit_solution(12754207814941976803)
XLA Ops:
  0.0 59.6 %shard_map.91 = bf16[8,8,16,128]{3,2,1,0:T(8,128)(2,1)S(1)} custom-call(s32[8,32]{1,0:T(8,128)} %chosen_in.1, bf16[8,8,16,128]{3,2,1,0:T(8,128)(2,1)} %bitcast.7, bf16[1024,128]{1,0:T(8,128)(2,1)} %latent_weight.1, bf16[1024,256]{1,0:T(8,128)(2,1)} %query_weight.1, bf16[128,1024]{1,0:T(8,128)(2,1)} %out_weight.1, f32[1,128]{1,0:T(1,128)} %bitcast.10, ...), custom_call_target="tpu_custom_call" | custom-call | tf_op jit(solution)/shard_map/pallas_call | solution.py:465
  59.6 0.7 %copy.11 = bf16[1024,128]{1,0:T(8,128)(2,1)} copy(bf16[1024,128]{1,0:T(8,128)(2,1)S(1)} %bitcast.6) | data formatting | bytes 524288

commit v11 on v10

--- a/solution.py
+++ b/solution.py
@@ -289,16 +289,16 @@
 
     def prepare(low, high):
         def several(j):
-            first = low + 4 * j
-            picked = [pool[:, first + i].reshape(BLOCK, width) for i in range(4)]
+            first = low + 8 * j
+            picked = [pool[:, first + i].reshape(BLOCK, width) for i in range(8)]
             turned = lax.dot_general(
                 eye, jnp.concatenate(picked, axis=0), (((1,), (1,)), ((), ())), preferred_element_type=jnp.float32
             ).astype(jnp.bfloat16)
-            for i in range(4):
+            for i in range(8):
                 keys[first + i] = unit(picked[i].astype(jnp.float32), key_gain[...])
                 values[first + i, :BLOCK, :] = turned[:, i * BLOCK : (i + 1) * BLOCK]
 
-        each(0, (high - low) // 4, several)
+        each(0, (high - low) // 8, several)
 
     wait_bytes(rows.at[pl.ds(0, peers - 1)], rows_send)
     token_spread.relay_first()
@@ -311,7 +311,11 @@
     token_spread.finish()
     own_query.wait()
     own_out.wait()
-    each(0, blocks, project)
+    def project_two(j):
+        project(2 * j)
+        project(2 * j + 1)
+
+    each(0, blocks // 2, project_two)
     for spread in spreads:
         spread.relay_first()
     out_spread = Spread(wide_weight, 0, 128, spread_send.at[2 + PIECES], spread_recv.at[2 + PIECES])

time: 60.4 us -> 58.7 us (0.972)
  Pallas kernels: 59.6 us -> 57.9 us
    pallas_call x1, Pallas kernels: 59.6 us -> 57.9 us  [shards(): pl.pallas_call(kernel, out_shape=pltpu.VMEM((blocks, peers, group, width)...]
where the time goes in v11:
time: 58.7 us; the launch traced here: 58.6 us
  Pallas kernels  57.9 us (99%)
  local copies, waits for them, and re-layouts  0.71 us (1%)
    pallas_call x1, Pallas kernels, shards(): pl.pallas_call(kernel, out_shape=pltpu.VMEM((blocks, peers, group, width)...  57.9 us

profile of v11, /device:TPU:1, one launch (start us, length us, event | category | flops | bytes accessed | tf_op | source)
XLA Modules:
  0.0 58.6 jit_solution(13968444393980672586)
XLA Ops:
  0.0 57.9 %shard_map.91 = bf16[8,8,16,128]{3,2,1,0:T(8,128)(2,1)S(1)} custom-call(s32[8,32]{1,0:T(8,128)} %chosen_in.1, bf16[8,8,16,128]{3,2,1,0:T(8,128)(2,1)} %bitcast.7, bf16[1024,128]{1,0:T(8,128)(2,1)} %latent_weight.1, bf16[1024,256]{1,0:T(8,128)(2,1)} %query_weight.1, bf16[128,1024]{1,0:T(8,128)(2,1)} %out_weight.1, f32[1,128]{1,0:T(1,128)} %bitcast.10, ...), custom_call_target="tpu_custom_call" | custom-call | tf_op jit(solution)/shard_map/pallas_call | solution.py:469
  57.9 0.7 %copy.11 = bf16[1024,128]{1,0:T(8,128)(2,1)} copy(bf16[1024,128]{1,0:T(8,128)(2,1)S(1)} %bitcast.6) | data formatting | bytes 524288

commit v12 on v11

--- a/solution.py
+++ b/solution.py
@@ -259,35 +259,44 @@
     each(0, others - kv, serve)
     low = pool.at[tp, pl.ds(0, PER_OWNER)]
     each(0, kv, lambda o: stay(low, served.at[o], serve_send))
-    each(kv, owners, lambda o: stay(low, serve_target(o), serve_recv.at[lax.div(o, share)]))
+    full_share = lax.div(kv + share - 1, share) * share
+    each(kv, full_share, lambda o: stay(low, serve_target(o), serve_recv.at[lax.div(o, share)]))
     here = Spread(pool, 0, blocks, spread_send.at[1], spread_recv.at[1])
     here.own()
 
+    per_piece = share * PER_OWNER
+    pieces = [lax.rem(lax.div(kv, share) + step, PIECES) for step in (0, 3, 1, 2)]
+    firsts = [blocks + piece * per_piece for piece in pieces]
     spreads = [
-        Spread(pool, blocks + i * share * PER_OWNER, share * PER_OWNER, spread_send.at[2 + i], spread_recv.at[2 + i])
-        for i in range(PIECES)
+        Spread(pool, first, per_piece, spread_send.at[2 + k], spread_recv.at[2 + k]) for k, first in enumerate(firsts)
     ]
 
-    def gathered(i):
-        per_piece = share * PER_OWNER
-        wait_bytes(pool.at[tp, pl.ds(blocks + i * per_piece, per_piece)], serve_recv.at[i])
-        spreads[i].start(0, 1)
+    def if_needed(k, act):
+        pl.when(pieces[k] * share < kv)(act)
+
+    def gathered(k):
+        wait_bytes(pool.at[tp, pl.ds(firsts[k], per_piece)], serve_recv.at[pieces[k]])
+        spreads[k].start(0, 1)
 
     scale = width ** (-0.5) * LOG2E
     query_row = query_gain[...] * scale
 
-    def project(b):
-        features = jnp.concatenate([full[p, b].reshape(BLOCK, width) for p in range(peers)], axis=1)
+    def project(j):
+        features = jnp.concatenate(
+            [full[p, pl.ds(2 * j, 2)].reshape(2 * BLOCK, width) for p in range(peers)], axis=1
+        )
         projected = jnp.dot(features, projection[...], preferred_element_type=jnp.float32)
         projected = projected.astype(jnp.bfloat16).astype(jnp.float32)
-        for h in range(up.shape[0]):
-            queries[b, h * BLOCK : (h + 1) * BLOCK, :] = unit(projected[:, h * 128 : (h + 1) * 128], query_row)
+        for i in range(2):
+            for h in range(up.shape[0]):
+                head = projected[i * BLOCK : (i + 1) * BLOCK, h * 128 : (h + 1) * 128]
+                queries[2 * j + i, h * BLOCK : (h + 1) * BLOCK, :] = unit(head, query_row)
 
     eye_shape = (BLOCK, BLOCK)
     same = lax.broadcasted_iota(jnp.int32, eye_shape, 0) == lax.broadcasted_iota(jnp.int32, eye_shape, 1)
     eye = jnp.where(same, 1.0, 0.0).astype(jnp.bfloat16)
 
-    def prepare(low, high):
+    def prepare(low, count):
         def several(j):
             first = low + 8 * j
             picked = [pool[:, first + i].reshape(BLOCK, width) for i in range(8)]
@@ -298,41 +307,37 @@
                 keys[first + i] = unit(picked[i].astype(jnp.float32), key_gain[...])
                 values[first + i, :BLOCK, :] = turned[:, i * BLOCK : (i + 1) * BLOCK]
 
-        each(0, (high - low) // 8, several)
+        each(0, count // 8, several)
 
     wait_bytes(rows.at[pl.ds(0, peers - 1)], rows_send)
     token_spread.relay_first()
     here.relay_first()
-    for i in range(PIECES):
-        gathered(i)
-    for spread in spreads:
-        spread.start(2, 3, 4, 5)
+    for k in range(PIECES):
+        if_needed(k, functools.partial(gathered, k))
+    for k in range(PIECES):
+        if_needed(k, functools.partial(spreads[k].start, 2, 3, 4, 5))
     token_spread.relay_rest()
     token_spread.finish()
     own_query.wait()
     own_out.wait()
-    def project_two(j):
-        project(2 * j)
-        project(2 * j + 1)
-
-    each(0, blocks // 2, project_two)
-    for spread in spreads:
-        spread.relay_first()
+    each(0, blocks // 2, project)
+    for k in range(PIECES):
+        if_needed(k, spreads[k].relay_first)
     out_spread = Spread(wide_weight, 0, 128, spread_send.at[2 + PIECES], spread_recv.at[2 + PIECES])
     out_spread.own()
     here.relay_rest()
     here.finish()
     prepare(0, blocks)
 
-    def complete(i):
-        spreads[i].finish()
-        prepare(blocks + i * share * PER_OWNER, blocks + (i + 1) * share * PER_OWNER)
-
-    spreads[0].relay_rest()
-    for i in range(1, PIECES):
-        spreads[i].relay_rest()
-        complete(i - 1)
-    complete(PIECES - 1)
+    def complete(k):
+        spreads[k].finish()
+        prepare(firsts[k], per_piece)
+
+    for k in range(PIECES + 1):
+        if k < PIECES:
+            if_needed(k, spreads[k].relay_rest)
+        if k > 0:
+            if_needed(k - 1, functools.partial(complete, k - 1))
     token_spread.drain()
 
     def heads_copy(to, b, slot):
@@ -378,6 +383,8 @@
         for side in range(sides):
             weigh(sides * i + side, side, 0)
 
+    groups = lax.div(jnp.minimum(picks, blocks + PER_OWNER * kv) + GROUP - 1, GROUP)
+
     def attend(i, following):
         first = sides * i
         for side in range(sides):
@@ -389,8 +396,10 @@
             for side in range(sides):
                 weigh(first + side, side, g)
 
-        each(1, picks // GROUP, both)
-        ended = [totals[side] + add_up(first + side, side, picks // GROUP - 1) for side in range(sides)]
+        each(1, groups, both)
+        if not following:
+            out_spread.relay_rest()
+        ended = [totals[side] + add_up(first + side, side, groups - 1) for side in range(sides)]
         if following:
             start(i + 1)
         hand_over(first, ended)
@@ -432,10 +441,6 @@
         def _():
             out_spread.relay_first()
 
-        @pl.when(i == 2)
-        def _():
-            out_spread.relay_rest()
-
     last = blocks // sides - 1
     each(0, 1, start)
     each(0, last, turn)
@@ -446,8 +451,10 @@
 
     wait_bytes(asks.at[pl.ds(0, others)], ask_send)
     wait_bytes(served.at[pl.ds(0, others)], serve_send)
-    for spread in (here, out_spread, *spreads):
+    for spread in (here, out_spread):
         spread.drain()
+    for k in range(PIECES):
+        if_needed(k, spreads[k].drain)
     wait_bytes(staged.at[:, pl.ds(0, peers - 1)], heads_send)
     wait_bytes(rows.at[pl.ds(0, peers - 1)], out_send)
     wait_bytes(out.at[:, pl.ds(0, peers - 1)], out_recv)

time: 58.7 us -> 54 us (0.920)
  the two profiles are of different devices: /device:TPU:1 before, /device:TPU:161 now
where the time goes in v12:
time: 54 us; the launch traced here: 53.9 us
  Pallas kernels  53.2 us (99%)
  local copies, waits for them, and re-layouts  0.71 us (1%)
    pallas_call x1, Pallas kernels, shards(): pl.pallas_call(kernel, out_shape=pltpu.VMEM((blocks, peers, group, width)...  53.2 us

profile of v12, /device:TPU:161, one launch (start us, length us, event | category | flops | bytes accessed | tf_op | source)
XLA Modules:
  0.0 53.9 jit_solution(14486001101251883406)
XLA Ops:
  0.0 53.2 %shard_map.91 = bf16[8,8,16,128]{3,2,1,0:T(8,128)(2,1)S(1)} custom-call(s32[8,32]{1,0:T(8,128)} %chosen_in.1, bf16[8,8,16,128]{3,2,1,0:T(8,128)(2,1)} %bitcast.7, bf16[1024,128]{1,0:T(8,128)(2,1)} %latent_weight.1, bf16[1024,256]{1,0:T(8,128)(2,1)} %query_weight.1, bf16[128,1024]{1,0:T(8,128)(2,1)} %out_weight.1, f32[1,128]{1,0:T(1,128)} %bitcast.10, ...), custom_call_target="tpu_custom_call" | custom-call | tf_op jit(solution)/shard_map/pallas_call | solution.py:476
  53.2 0.7 %copy.11 = bf16[1024,128]{1,0:T(8,128)(2,1)} copy(bf16[1024,128]{1,0:T(8,128)(2,1)S(1)} %bitcast.6) | data formatting | bytes 524288

commit v13 on v12

--- a/solution.py
+++ b/solution.py
@@ -312,15 +312,23 @@
     wait_bytes(rows.at[pl.ds(0, peers - 1)], rows_send)
     token_spread.relay_first()
     here.relay_first()
-    for k in range(PIECES):
-        if_needed(k, functools.partial(gathered, k))
-    for k in range(PIECES):
-        if_needed(k, functools.partial(spreads[k].start, 2, 3, 4, 5))
+    near = kv >= owners - share
+
+    def far_pieces():
+        for k in range(1, PIECES):
+            if_needed(k, functools.partial(gathered, k))
+        for k in range(1, PIECES):
+            if_needed(k, functools.partial(spreads[k].start, 2, 3, 4, 5))
+
+    if_needed(0, functools.partial(gathered, 0))
+    if_needed(0, functools.partial(spreads[0].start, 2, 3, 4, 5))
+    pl.when(near)(far_pieces)
     token_spread.relay_rest()
     token_spread.finish()
     own_query.wait()
     own_out.wait()
     each(0, blocks // 2, project)
+    pl.when(jnp.logical_not(near))(far_pieces)
     for k in range(PIECES):
         if_needed(k, spreads[k].relay_first)
     out_spread = Spread(wide_weight, 0, 128, spread_send.at[2 + PIECES], spread_recv.at[2 + PIECES])

time: 54 us -> 55.5 us (1.028)
  the two profiles are of different devices: /device:TPU:161 before, /device:TPU:97 now
where the time goes in v13:
time: 55.5 us; the launch traced here: 55.4 us
  Pallas kernels  54.7 us (99%)
  local copies, waits for them, and re-layouts  0.71 us (1%)
    pallas_call x1, Pallas kernels, shards(): pl.pallas_call(kernel, out_shape=pltpu.VMEM((blocks, peers, group, width)...  54.7 us

profile of v13, /device:TPU:97, one launch (start us, length us, event | category | flops | bytes accessed | tf_op | source)
XLA Modules:
  0.0 55.4 jit_solution(5971596805419538263)
XLA Ops:
  0.0 54.7 %shard_map.91 = bf16[8,8,16,128]{3,2,1,0:T(8,128)(2,1)S(1)} custom-call(s32[8,32]{1,0:T(8,128)} %chosen_in.1, bf16[8,8,16,128]{3,2,1,0:T(8,128)(2,1)} %bitcast.7, bf16[1024,128]{1,0:T(8,128)(2,1)} %latent_weight.1, bf16[1024,256]{1,0:T(8,128)(2,1)} %query_weight.1, bf16[128,1024]{1,0:T(8,128)(2,1)} %out_weight.1, f32[1,128]{1,0:T(1,128)} %bitcast.10, ...), custom_call_target="tpu_custom_call" | custom-call | tf_op jit(solution)/shard_map/pallas_call | solution.py:484
  54.7 0.7 %copy.11 = bf16[1024,128]{1,0:T(8,128)(2,1)} copy(bf16[1024,128]{1,0:T(8,128)(2,1)S(1)} %bitcast.6) | data formatting | bytes 524288

commit v14 on v13

--- a/solution.py
+++ b/solution.py
@@ -312,7 +312,7 @@
     wait_bytes(rows.at[pl.ds(0, peers - 1)], rows_send)
     token_spread.relay_first()
     here.relay_first()
-    near = kv >= owners - share
+    near = jnp.logical_or(kv >= owners - share, kv < owners // 2)
 
     def far_pieces():
         for k in range(1, PIECES):
@@ -328,12 +328,12 @@
     own_query.wait()
     own_out.wait()
     each(0, blocks // 2, project)
+    here.relay_rest()
     pl.when(jnp.logical_not(near))(far_pieces)
     for k in range(PIECES):
         if_needed(k, spreads[k].relay_first)
     out_spread = Spread(wide_weight, 0, 128, spread_send.at[2 + PIECES], spread_recv.at[2 + PIECES])
     out_spread.own()
-    here.relay_rest()
     here.finish()
     prepare(0, blocks)
 

time: 55.5 us -> 53.5 us (0.964)
  Pallas kernels: 54.7 us -> 52.7 us
    pallas_call x1, Pallas kernels: 54.7 us -> 52.7 us  [shards(): pl.pallas_call(kernel, out_shape=pltpu.VMEM((blocks, peers, group, width)...]
where the time goes in v14:
time: 53.5 us; the launch traced here: 53.4 us
  Pallas kernels  52.7 us (99%)
  local copies, waits for them, and re-layouts  0.71 us (1%)
    pallas_call x1, Pallas kernels, shards(): pl.pallas_call(kernel, out_shape=pltpu.VMEM((blocks, peers, group, width)...  52.7 us

profile of v14, /device:TPU:97, one launch (start us, length us, event | category | flops | bytes accessed | tf_op | source)
XLA Modules:
  0.0 53.4 jit_solution(1559219832754157490)
XLA Ops:
  0.0 52.7 %shard_map.91 = bf16[8,8,16,128]{3,2,1,0:T(8,128)(2,1)S(1)} custom-call(s32[8,32]{1,0:T(8,128)} %chosen_in.1, bf16[8,8,16,128]{3,2,1,0:T(8,128)(2,1)} %bitcast.7, bf16[1024,128]{1,0:T(8,128)(2,1)} %latent_weight.1, bf16[1024,256]{1,0:T(8,128)(2,1)} %query_weight.1, bf16[128,1024]{1,0:T(8,128)(2,1)} %out_weight.1, f32[1,128]{1,0:T(1,128)} %bitcast.10, ...), custom_call_target="tpu_custom_call" | custom-call | tf_op jit(solution)/shard_map/pallas_call | solution.py:484
  52.7 0.7 %copy.11 = bf16[1024,128]{1,0:T(8,128)(2,1)} copy(bf16[1024,128]{1,0:T(8,128)(2,1)S(1)} %bitcast.6) | data formatting | bytes 524288

commit v15 on v14

--- a/solution.py
+++ b/solution.py
@@ -404,9 +404,12 @@
             for side in range(sides):
                 weigh(first + side, side, g)
 
-        each(1, groups, both)
-        if not following:
+        if following:
+            each(1, groups, both)
+        else:
+            each(1, jnp.minimum(groups, 2), both)
             out_spread.relay_rest()
+            each(2, groups, both)
         ended = [totals[side] + add_up(first + side, side, groups - 1) for side in range(sides)]
         if following:
             start(i + 1)

time: 53.5 us -> 53.8 us (level)
  the two profiles are of different devices: /device:TPU:97 before, /device:TPU:161 now
where the time goes in v15:
time: 53.8 us; the launch traced here: 53.7 us
  Pallas kernels  53 us (99%)
  local copies, waits for them, and re-layouts  0.71 us (1%)
    pallas_call x1, Pallas kernels, shards(): pl.pallas_call(kernel, out_shape=pltpu.VMEM((blocks, peers, group, width)...  53 us

profile of v15, /device:TPU:161, one launch (start us, length us, event | category | flops | bytes accessed | tf_op | source)
XLA Modules:
  0.0 53.7 jit_solution(3816992811742640081)
XLA Ops:
  0.0 53.0 %shard_map.91 = bf16[8,8,16,128]{3,2,1,0:T(8,128)(2,1)S(1)} custom-call(s32[8,32]{1,0:T(8,128)} %chosen_in.1, bf16[8,8,16,128]{3,2,1,0:T(8,128)(2,1)} %bitcast.7, bf16[1024,128]{1,0:T(8,128)(2,1)} %latent_weight.1, bf16[1024,256]{1,0:T(8,128)(2,1)} %query_weight.1, bf16[128,1024]{1,0:T(8,128)(2,1)} %out_weight.1, f32[1,128]{1,0:T(1,128)} %bitcast.10, ...), custom_call_target="tpu_custom_call" | custom-call | tf_op jit(solution)/shard_map/pallas_call | solution.py:487
  53.0 0.7 %copy.11 = bf16[1024,128]{1,0:T(8,128)(2,1)} copy(bf16[1024,128]{1,0:T(8,128)(2,1)S(1)} %bitcast.6) | data formatting | bytes 524288

commit v16 on v15

--- a/solution.py
+++ b/solution.py
@@ -14,6 +14,7 @@
 PIECES = 4
 ONES = 16
 HALF = 6
+GROUPS_EARLY = 3
 LOG2E = 1.4426950408889634
 
 
@@ -404,12 +405,13 @@
             for side in range(sides):
                 weigh(first + side, side, g)
 
+        early = jnp.minimum(groups, GROUPS_EARLY)
+        each(1, early, both)
         if following:
-            each(1, groups, both)
+            pl.when(i == 0)(out_spread.relay_first)
         else:
-            each(1, jnp.minimum(groups, 2), both)
             out_spread.relay_rest()
-            each(2, groups, both)
+        each(early, groups, both)
         ended = [totals[side] + add_up(first + side, side, groups - 1) for side in range(sides)]
         if following:
             start(i + 1)
@@ -447,10 +449,6 @@
 
     def turn(i):
         attend(i, True)
-
-        @pl.when(i == 0)
-        def _():
-            out_spread.relay_first()
 
     last = blocks // sides - 1
     each(0, 1, start)

time: 53.8 us -> 53.5 us (level)
  the two profiles are of different devices: /device:TPU:161 before, /device:TPU:97 now
where the time goes in v16:
time: 53.5 us; the launch traced here: 53.4 us
  Pallas kernels  52.7 us (99%)
  local copies, waits for them, and re-layouts  0.71 us (1%)
    pallas_call x1, Pallas kernels, shards(): pl.pallas_call(kernel, out_shape=pltpu.VMEM((blocks, peers, group, width)...  52.7 us

profile of v16, /device:TPU:97, one launch (start us, length us, event | category | flops | bytes accessed | tf_op | source)
XLA Modules:
  0.0 53.4 jit_solution(8414432813915860557)
XLA Ops:
  0.0 52.7 %shard_map.91 = bf16[8,8,16,128]{3,2,1,0:T(8,128)(2,1)S(1)} custom-call(s32[8,32]{1,0:T(8,128)} %chosen_in.1, bf16[8,8,16,128]{3,2,1,0:T(8,128)(2,1)} %bitcast.7, bf16[1024,128]{1,0:T(8,128)(2,1)} %latent_weight.1, bf16[1024,256]{1,0:T(8,128)(2,1)} %query_weight.1, bf16[128,1024]{1,0:T(8,128)(2,1)} %out_weight.1, f32[1,128]{1,0:T(1,128)} %bitcast.10, ...), custom_call_target="tpu_custom_call" | custom-call | tf_op jit(solution)/shard_map/pallas_call | solution.py:485
  52.7 0.7 %copy.11 = bf16[1024,128]{1,0:T(8,128)(2,1)} copy(bf16[1024,128]{1,0:T(8,128)(2,1)S(1)} %bitcast.6) | data formatting | bytes 524288

commit v17 on v16

--- a/solution.py
+++ b/solution.py
@@ -14,6 +14,7 @@
 PIECES = 4
 ONES = 16
 HALF = 6
+LAYERS = 8
 GROUPS_EARLY = 3
 LOG2E = 1.4426950408889634
 
@@ -246,8 +247,7 @@
     pool[tp, 0:blocks] = latent
     latent = latent.astype(jnp.float32)
 
-    def serve(i):
-        r = others - i
+    def serve(r):
         for k in range(PER_OWNER):
             want = asked[r, k : k + 1, :]
             picked = jnp.zeros((group, 128), jnp.float32)
@@ -256,8 +256,14 @@
             served[r, k] = picked.astype(jnp.bfloat16)
         serve_copy(r, kv).start()
 
+    def serve_in_turn(n):
+        turn = lax.rem(n, LAYERS)
+        away = lax.div(turn + 1, 2) * (2 * lax.rem(turn, 2) - 1)
+        r = lax.rem(LAYERS // 2 + away, LAYERS) * (owners // LAYERS) + lax.div(n, LAYERS)
+        pl.when(r > kv)(lambda: serve(r))
+
     wait_bytes(asked.at[pl.ds(0, others)], ask_recv)
-    each(0, others - kv, serve)
+    each(0, owners, serve_in_turn)
     low = pool.at[tp, pl.ds(0, PER_OWNER)]
     each(0, kv, lambda o: stay(low, served.at[o], serve_send))
     full_share = lax.div(kv + share - 1, share) * share

time: 53.5 us -> 53.6 us (level)
  the two profiles are of different devices: /device:TPU:97 before, /device:TPU:161 now
where the time goes in v17:
time: 53.6 us; the launch traced here: 53.5 us
  Pallas kernels  52.8 us (99%)
  local copies, waits for them, and re-layouts  0.71 us (1%)
    pallas_call x1, Pallas kernels, shards(): pl.pallas_call(kernel, out_shape=pltpu.VMEM((blocks, peers, group, width)...  52.8 us

profile of v17, /device:TPU:161, one launch (start us, length us, event | category | flops | bytes accessed | tf_op | source)
XLA Modules:
  0.0 53.5 jit_solution(5963853206425246942)
XLA Ops:
  0.0 52.8 %shard_map.91 = bf16[8,8,16,128]{3,2,1,0:T(8,128)(2,1)S(1)} custom-call(s32[8,32]{1,0:T(8,128)} %chosen_in.1, bf16[8,8,16,128]{3,2,1,0:T(8,128)(2,1)} %bitcast.7, bf16[1024,128]{1,0:T(8,128)(2,1)} %latent_weight.1, bf16[1024,256]{1,0:T(8,128)(2,1)} %query_weight.1, bf16[128,1024]{1,0:T(8,128)(2,1)} %out_weight.1, f32[1,128]{1,0:T(1,128)} %bitcast.10, ...), custom_call_target="tpu_custom_call" | custom-call | tf_op jit(solution)/shard_map/pallas_call | solution.py:491
  52.8 0.7 %copy.11 = bf16[1024,128]{1,0:T(8,128)(2,1)} copy(bf16[1024,128]{1,0:T(8,128)(2,1)S(1)} %bitcast.6) | data formatting | bytes 524288

commit v18 on v17

--- a/solution.py
+++ b/solution.py
@@ -319,8 +319,6 @@
     wait_bytes(rows.at[pl.ds(0, peers - 1)], rows_send)
     token_spread.relay_first()
     here.relay_first()
-    near = jnp.logical_or(kv >= owners - share, kv < owners // 2)
-
     def far_pieces():
         for k in range(1, PIECES):
             if_needed(k, functools.partial(gathered, k))
@@ -329,14 +327,13 @@
 
     if_needed(0, functools.partial(gathered, 0))
     if_needed(0, functools.partial(spreads[0].start, 2, 3, 4, 5))
-    pl.when(near)(far_pieces)
+    far_pieces()
     token_spread.relay_rest()
     token_spread.finish()
     own_query.wait()
     own_out.wait()
     each(0, blocks // 2, project)
     here.relay_rest()
-    pl.when(jnp.logical_not(near))(far_pieces)
     for k in range(PIECES):
         if_needed(k, spreads[k].relay_first)
     out_spread = Spread(wide_weight, 0, 128, spread_send.at[2 + PIECES], spread_recv.at[2 + PIECES])

time: 53.6 us -> 53.5 us (level)
  the two profiles are of different devices: /device:TPU:161 before, /device:TPU:217 now
where the time goes in v18:
time: 53.5 us; the launch traced here: 53.4 us
  Pallas kernels  52.7 us (99%)
  local copies, waits for them, and re-layouts  0.71 us (1%)
    pallas_call x1, Pallas kernels, shards(): pl.pallas_call(kernel, out_shape=pltpu.VMEM((blocks, peers, group, width)...  52.7 us

profile of v18, /device:TPU:217, one launch (start us, length us, event | category | flops | bytes accessed | tf_op | source)
XLA Modules:
  0.0 53.4 jit_solution(7720028112831940344)
XLA Ops:
  0.0 52.7 %shard_map.91 = bf16[8,8,16,128]{3,2,1,0:T(8,128)(2,1)S(1)} custom-call(s32[8,32]{1,0:T(8,128)} %chosen_in.1, bf16[8,8,16,128]{3,2,1,0:T(8,128)(2,1)} %bitcast.7, bf16[1024,128]{1,0:T(8,128)(2,1)} %latent_weight.1, bf16[1024,256]{1,0:T(8,128)(2,1)} %query_weight.1, bf16[128,1024]{1,0:T(8,128)(2,1)} %out_weight.1, f32[1,128]{1,0:T(1,128)} %bitcast.10, ...), custom_call_target="tpu_custom_call" | custom-call | tf_op jit(solution)/shard_map/pallas_call | solution.py:488
  52.7 0.7 %copy.11 = bf16[1024,128]{1,0:T(8,128)(2,1)} copy(bf16[1024,128]{1,0:T(8,128)(2,1)S(1)} %bitcast.6) | data formatting | bytes 524288

commit v19 on v17

--- a/solution.py
+++ b/solution.py
@@ -43,7 +43,7 @@
         me, right, left, far, other = self.tp, self.right, self.left, self.far, self.other
         return (
             (me, 0, right, 0), (me, 1, left, 0), (me, 1, right, 1), (me, 0, left, 1), (me, 0, other, 2), (me, 1, other, 2),
-            (left, 0, right, 1), (right, 1, left, 1), (left, 0, other, 2), (right, 1, other, 2), (left, 1, other, 2),
+            (left, 0, right, 3), (right, 1, left, 3), (left, 0, other, 2), (right, 1, other, 2), (left, 1, other, 2),
             (right, 0, other, 2), (far, 0, other, 2), (far, 1, other, 2),
         )
 
@@ -65,9 +65,17 @@
         self.slices(1, self.recv_sem.at[0])
         self.start(6, 7, 8, 9)
 
+    def relay_near(self):
+        self.slices(1, self.recv_sem.at[1])
+        self.start(10, 11)
+
+    def relay_far(self):
+        self.slices(1, self.recv_sem.at[3])
+        self.start(12, 13)
+
     def relay_rest(self):
-        self.slices(2, self.recv_sem.at[1])
-        self.start(10, 11, 12, 13)
+        self.relay_near()
+        self.relay_far()
 
     def finish(self):
         self.slices(4, self.recv_sem.at[2])
@@ -318,6 +326,7 @@
 
     wait_bytes(rows.at[pl.ds(0, peers - 1)], rows_send)
     token_spread.relay_first()
+    token_spread.relay_near()
     here.relay_first()
     near = jnp.logical_or(kv >= owners - share, kv < owners // 2)
 
@@ -330,7 +339,7 @@
     if_needed(0, functools.partial(gathered, 0))
     if_needed(0, functools.partial(spreads[0].start, 2, 3, 4, 5))
     pl.when(near)(far_pieces)
-    token_spread.relay_rest()
+    token_spread.relay_far()
     token_spread.finish()
     own_query.wait()
     own_out.wait()
@@ -524,7 +533,7 @@
             dma, dma((PIECES,)),
             dma, dma((2,)),
             dma, dma,
-            dma((3 + PIECES,)), dma((3 + PIECES, 3)),
+            dma((3 + PIECES,)), dma((3 + PIECES, 4)),
         ],
         compiler_params=pltpu.CompilerParams(collective_id=0, has_side_effects=True),
     )(

time: 53.6 us -> 53.3 us (level)
  no operation moved by 1% of the time
where the time goes in v19:
time: 53.3 us; the launch traced here: 53.2 us
  Pallas kernels  52.5 us (98%)
  local copies, waits for them, and re-layouts  0.71 us (1%)
    pallas_call x1, Pallas kernels, shards(): pl.pallas_call(kernel, out_shape=pltpu.VMEM((blocks, peers, group, width)...  52.5 us

profile of v19, /device:TPU:161, one launch (start us, length us, event | category | flops | bytes accessed | tf_op | source)
XLA Modules:
  0.0 53.2 jit_solution(18241020575128597054)
XLA Ops:
  0.0 52.5 %shard_map.91 = bf16[8,8,16,128]{3,2,1,0:T(8,128)(2,1)S(1)} custom-call(s32[8,32]{1,0:T(8,128)} %chosen_in.1, bf16[8,8,16,128]{3,2,1,0:T(8,128)(2,1)} %bitcast.7, bf16[1024,128]{1,0:T(8,128)(2,1)} %latent_weight.1, bf16[1024,256]{1,0:T(8,128)(2,1)} %query_weight.1, bf16[128,1024]{1,0:T(8,128)(2,1)} %out_weight.1, f32[1,128]{1,0:T(1,128)} %bitcast.10, ...), custom_call_target="tpu_custom_call" | custom-call | tf_op jit(solution)/shard_map/pallas_call | solution.py:500
  52.5 0.7 %copy.11 = bf16[1024,128]{1,0:T(8,128)(2,1)} copy(bf16[1024,128]{1,0:T(8,128)(2,1)S(1)} %bitcast.6) | data formatting | bytes 524288

commit v20 on v19

--- a/solution.py
+++ b/solution.py
@@ -171,7 +171,8 @@
         return remote(served.at[to], serve_target(slot), serve_send, serve_recv.at[lax.div(slot, share)], "kv", to)
 
     def peer(i):
-        return lax.rem(tp + i, peers)
+        away = lax.div(i, 2) * (1 - 2 * lax.rem(i, 2))
+        return lax.rem(tp + peers // 2 + away, peers)
 
     each(1, peers, lambda i: rows_copy(peer(i), tp).start())
     token_spread = Spread(

time: 53.3 us -> 53.2 us (level)
  the two profiles are of different devices: /device:TPU:161 before, /device:TPU:129 now
where the time goes in v20:
time: 53.2 us; the launch traced here: 53.1 us
  Pallas kernels  52.4 us (98%)
  local copies, waits for them, and re-layouts  0.71 us (1%)
    pallas_call x1, Pallas kernels, shards(): pl.pallas_call(kernel, out_shape=pltpu.VMEM((blocks, peers, group, width)...  52.4 us

profile of v20, /device:TPU:129, one launch (start us, length us, event | category | flops | bytes accessed | tf_op | source)
XLA Modules:
  0.0 53.1 jit_solution(3941657572092020232)
XLA Ops:
  0.0 52.4 %shard_map.91 = bf16[8,8,16,128]{3,2,1,0:T(8,128)(2,1)S(1)} custom-call(s32[8,32]{1,0:T(8,128)} %chosen_in.1, bf16[8,8,16,128]{3,2,1,0:T(8,128)(2,1)} %bitcast.7, bf16[1024,128]{1,0:T(8,128)(2,1)} %latent_weight.1, bf16[1024,256]{1,0:T(8,128)(2,1)} %query_weight.1, bf16[128,1024]{1,0:T(8,128)(2,1)} %out_weight.1, f32[1,128]{1,0:T(1,128)} %bitcast.10, ...), custom_call_target="tpu_custom_call" | custom-call | tf_op jit(solution)/shard_map/pallas_call | solution.py:501
  52.4 0.7 %copy.11 = bf16[1024,128]{1,0:T(8,128)(2,1)} copy(bf16[1024,128]{1,0:T(8,128)(2,1)S(1)} %bitcast.6) | data formatting | bytes 524288
